TPU v7x, 32 devices: a whole 2x2x4 slice. The times are simulated.
32 devices in a mesh: sp: 8 (over z, x), tp: 4 (over y, core).
Axes of the slice: x: 2, y: 2, z: 4, core: 2. Of those that a mesh axis runs over, the one named last changes fastest.
Arguments:
- tokens: bfloat16 [3072, 2048], P('sp'), may hold values from -6 to 6
- doc_ids: int32 [3072], P('sp'), may hold values from 0 to 2, never falling along the last dimension, each value on 1 to 2048 neighbouring positions
- pre_gain: float32 [2, 2048], replicated, may hold values from 0.1 to 1.9
- value_proj: bfloat16 [2, 2048, 1024], P(None, 'sp', 'tp'), may hold values from -0.1875 to 0.1875
- gate_proj: bfloat16 [2, 2048, 1024], P(None, 'sp', 'tp'), may hold values from -0.1875 to 0.1875
- out_proj: bfloat16 [2, 1024, 2048], P(None, 'tp', 'sp'), may hold values from -0.1875 to 0.1875
- conv_taps: float32 [2, 31, 1024], P(None, None, 'tp'), may hold values from -2.2 to 2.2
- norm_gain: float32 [2, 1024], P(None, 'tp'), may hold values from 0.1 to 1.9
- norm_shift: float32 [2, 1024], P(None, 'tp'), may hold values from -3 to 3
Outputs:
- hidden: bfloat16 [3072, 2048], P('sp')
Inputs may be any that keep to these rules, and one draw needn't show every extreme that they name: `doc_ids`: document numbers never fall along the sequence; each document has 1 to 2048 positions.
All inputs are finite; a program needn't handle non-finite values.
Results may differ from a plain program's by a relative error of at most 0.017.
Values may be sent and summed in bfloat16 or wider, within the bound.
A program may use at most 64 MiB of HBM per device.

v0:
```python
import functools
import jax
import jax.numpy as jnp
from jax import lax
from jax.experimental import pallas as pl
from jax.experimental.pallas import tpu as pltpu
from jax.sharding import PartitionSpec as P

epsilon = 1e-06
MESH = pl.DeviceIdType.MESH
HALO = 32
CONV_ROWS = 64


def fused_kernel(
    n, m, reach, layers,
    tok_ref, doc_ref, gain_ref, v_ref, g_ref, o_ref, tap_ref, ng_ref, ns_ref,
    out_ref,
    w, oring, ofull, normed, acc, padded, pdoc, run, ghalo, halo_in, doc_in, doc_tail,
    stat, stat_out, stat_in, conv, act_all, hid,
    rsend, rrecv, osend, orecv, hsend, hrecv, ssend, srecv, asend, arecv, xsend, xrecv,
):
    me = lax.axis_index("sp")
    t = lax.axis_index("tp")
    q, c = t // 2, t % 2
    pairs = m // 2
    half_n = n // 2
    rows, width = tok_ref.shape
    depth, block = v_ref.shape[1], v_ref.shape[2]
    owidth = o_ref.shape[2]
    hd, ho = depth // 2, owidth // 2
    half_width = width // 2
    channels = block * m

    def index_of(position):
        position = (position + 2 * n) % n
        return jnp.where(position < half_n, 2 * position, 2 * (n - 1 - position) + 1)

    my_pos = jnp.where(me % 2 == 0, me // 2, n - 1 - me // 2)
    right, left = index_of(my_pos + 1), index_of(my_pos - 1)
    following, before = (me + 1) % n, (me + n - 1) % n

    barrier = pltpu.get_barrier_semaphore()
    for other in (right, left, following, before):
        pl.semaphore_signal(barrier, inc=1, device_id={"sp": other}, device_id_type=MESH)
    for k in range(1, m):
        pl.semaphore_signal(barrier, inc=1, device_id={"tp": (t + k) % m}, device_id_type=MESH)
    pl.semaphore_wait(barrier, 3 + m)

    def to_sp(src, dst, send, recv, target):
        return pltpu.make_async_remote_copy(
            src_ref=src, dst_ref=dst, send_sem=send, recv_sem=recv,
            device_id={"sp": target}, device_id_type=MESH)

    def to_tp(src, dst, send, recv, target):
        return pltpu.make_async_remote_copy(
            src_ref=src, dst_ref=dst, send_sem=send, recv_sem=recv,
            device_id={"tp": target}, device_id_type=MESH)

    def w_piece(layer, owner, way, part):
        return w.at[layer, pl.ds(pl.multiple_of(owner * depth + part * hd, hd), hd),
                    pl.ds(way * block, block)]

    def o_piece(layer, owner, way):
        return oring.at[layer, :, pl.ds(pl.multiple_of(owner * owidth + way * ho, ho), ho)]

    def ring_copy(layer, msg, way, step, own=False):
        owner = index_of(my_pos - step if way == 0 else my_pos + step)
        if msg < 2:
            dst = w_piece(layer, owner, way, msg)
            src = (v_ref, g_ref)[way].at[layer, pl.ds(msg * hd, hd), :] if own else dst
        else:
            dst = o_piece(layer, owner, way)
            src = o_ref.at[layer, :, pl.ds(way * ho, ho)] if own else dst
        return to_sp(src, dst, rsend.at[layer, msg, way, step], rrecv.at[layer, msg, way, step],
                     right if way == 0 else left)

    def arrival(layer, msg, way, step):
        owner = index_of(my_pos - step - 1 if way == 0 else my_pos + step + 1)
        dst = w_piece(layer, owner, way, msg) if msg < 2 else o_piece(layer, owner, way)
        return to_sp(dst, dst, rsend.at[layer, msg, way, step], rrecv.at[layer, msg, way, step],
                     right if way == 0 else left)

    def spread_copy(layer, way, step, pair, own=False):
        owner = index_of(my_pos - step if way == 0 else my_pos + step)
        part = owner // half_n
        local = owner - part * half_n
        src = o_ref.at[layer, :, pl.ds(way * ho, ho)] if own else o_piece(layer, owner, way)
        dst = ofull.at[layer, pl.ds(pl.multiple_of(t * block, block), block),
                       pl.ds(pl.multiple_of(local * owidth + way * ho, ho), ho)]
        copy = to_tp(src, dst, osend.at[layer, way, step, pair],
                     orecv.at[layer, t, local * 2 + way], 2 * ((q + pair) % pairs) + part)
        return copy, part

    def spread(layer, way, step, act, own=False):
        for pair in range(pairs - 1, -1, -1):
            copy, part = spread_copy(layer, way, step, pair, own)
            if pair == 0:
                pl.when(part != c)(lambda copy=copy: getattr(copy, act)())
            else:
                getattr(copy, act)()

    def slot(time):
        for layer in reversed(range(layers)):
            step = time - (n - 1) * layer
            if not 0 <= step <= n - 1:
                continue
            for msg in range(3):
                for way in range(2):
                    if step > 0:
                        arrival(layer, msg, way, step - 1).wait_recv()
                    if step < n - 1:
                        ring_copy(layer, msg, way, step, own=step == 0).start()
            for way in range(2):
                spread(layer, way, step, "start", own=step == 0)

    def keep_own(layer):
        row = pl.ds(pl.multiple_of(me * depth, depth), depth)
        w[layer, row, pl.ds(0, block)] = v_ref[layer]
        w[layer, row, pl.ds(block, block)] = g_ref[layer]
        oring[layer, :, pl.ds(pl.multiple_of(me * owidth, owidth), owidth)] = o_ref[layer]

    slot(0)

    def doc_block(i):
        row = doc_ref[pl.ds(i, 1), :].astype(jnp.float32)
        return jnp.transpose(jnp.broadcast_to(row, (128, 128)))

    doc_tail[...] = doc_block(rows // 128 - 1)[128 - HALO:]
    doc_copy = to_sp(doc_tail, doc_in, hsend.at[layers],
                     hrecv.at[layers], following)
    doc_copy.start()

    for i in range(rows // 128):
        pdoc[pl.ds(HALO + i * 128, 128), :] = doc_block(i)

    def norm_rows(layer, source):
        @pl.loop(0, rows // 32)
        def _(i):
            span = pl.ds(pl.multiple_of(i * 32, 32), 32)
            wide = source[span, :].astype(jnp.float32)
            scale = lax.rsqrt(jnp.mean(wide * wide, axis=-1, keepdims=True) + epsilon)
            normed[span, :] = (wide * scale * gain_ref[pl.ds(layer, 1), :]).astype(jnp.bfloat16)

    norm_rows(0, tok_ref)
    keep_own(0)
    slot(1)
    doc_copy.wait_recv()
    pdoc[pl.ds(0, HALO), :] = jnp.where(me == 0, jnp.float32(-1.0), doc_in[...])

    @pl.loop(0, rows // CONV_ROWS)
    def _(i):
        base = pl.multiple_of(i * CONV_ROWS, CONV_ROWS)
        mine = pdoc[pl.ds(base + HALO, CONV_ROWS), :]
        count = jnp.zeros((CONV_ROWS, 128), jnp.int32)
        for j in range(1, reach + 1):
            count = count + (pdoc[pl.ds(base + (HALO - j), CONV_ROWS), :] == mine).astype(jnp.int32)
        run[pl.ds(base, CONV_ROWS), :] = count

    for later in range(1, layers):
        keep_own(later)
    for time in range(2, n):
        slot(time)

    lane = lax.broadcasted_iota(jnp.int32, (CONV_ROWS, 128), 1)

    def layer_step(layer, source, target):
        nxt = layer + 1 if layer + 1 < layers else None
        opened = (n - 1) * (layer + 1) + 1
        times = list(range(opened, opened + n - 1)) if nxt is not None else []
        shares = [times[i:i + 1] for i in range(6)] + [times[6:]]

        def tend():
            for time in shares.pop(0):
                slot(time)

        acc[...] = jnp.dot(normed[...], w[layer], preferred_element_type=jnp.float32)

        def store_padded(row, values):
            for part in range(block // 128):
                padded[pl.ds(row + part * (rows + HALO), 32), :] = values[:, part * 128:(part + 1) * 128].astype(jnp.float32)

        def gate_rows(i):
            span = pl.ds(pl.multiple_of(i * 32, 32), 32)
            value = acc[span, pl.ds(0, block)].astype(jnp.bfloat16).astype(jnp.float32)
            gate = acc[span, pl.ds(block, block)].astype(jnp.bfloat16).astype(jnp.float32)
            gated = (value * jax.nn.sigmoid(gate)).astype(jnp.bfloat16)
            store_padded(pl.multiple_of(i * 32 + HALO, 32), gated)
            return gated

        ghalo[layer] = gate_rows(rows // 32 - 1)
        halo_copy = to_sp(ghalo.at[layer], halo_in.at[layer], hsend.at[layer], hrecv.at[layer], following)
        halo_copy.start()

        @pl.loop(0, rows // 32 - 1)
        def _(i):
            gate_rows(i)

        tend()
        halo_copy.wait_recv()
        store_padded(0, halo_in[layer])

        def conv_rows(i):
            base = pl.multiple_of(i * CONV_ROWS, CONV_ROWS)
            count = run[pl.ds(base, CONV_ROWS), :]
            first_sum = jnp.zeros((CONV_ROWS, 1), jnp.float32)
            square_sum = jnp.zeros((CONV_ROWS, 1), jnp.float32)
            for part in range(block // 128):
                cols = pl.ds(part * 128, 128)
                lift = part * (rows + HALO)
                total = tap_ref[0, pl.ds(layer, 1), cols] * padded[pl.ds(base + (lift + HALO), CONV_ROWS), :]
                for j in range(1, reach + 1):
                    term = tap_ref[j, pl.ds(layer, 1), cols] * padded[pl.ds(base + (lift + HALO - j), CONV_ROWS), :]
                    total = total + jnp.where(count >= j, term, jnp.float32(0.0))
                conv[pl.ds(base, CONV_ROWS), cols] = total
                first_sum = first_sum + jnp.sum(total, axis=1, keepdims=True)
                square_sum = square_sum + jnp.sum(total * total, axis=1, keepdims=True)
            stat[pl.ds(base, CONV_ROWS), :] = jnp.where(
                lane == 0, first_sum, jnp.where(lane == 1, square_sum, jnp.float32(0.0)))

        middle = rows // CONV_ROWS // 2
        pl.loop(0, middle)(conv_rows)
        tend()
        pl.loop(middle, rows // CONV_ROWS)(conv_rows)
        stat_out[layer] = jnp.transpose(stat[...])[:8]
        stat_copies = [
            to_tp(stat_out.at[layer], stat_in.at[layer, t], ssend.at[layer, k], srecv.at[layer, t], (t + k) % m)
            for k in range(1, m)]
        for copy in stat_copies:
            copy.start()
        tend()
        summed = stat_out[layer]
        for k in range(1, m):
            peer = (t + k) % m
            to_tp(stat_in.at[layer, peer], stat_in.at[layer, peer], ssend.at[layer, k],
                  srecv.at[layer, peer], peer).wait_recv()
            summed = summed + stat_in[layer, peer]
        stat[...] = jnp.transpose(
            jnp.concatenate([summed, jnp.zeros((120, rows), jnp.float32)], axis=0))

        mine = pl.ds(pl.multiple_of(t * block, block), block)

        @pl.loop(0, rows // CONV_ROWS)
        def _(i):
            span = pl.ds(pl.multiple_of(i * CONV_ROWS, CONV_ROWS), CONV_ROWS)
            both = stat[span, :]
            row_mean = both[:, 0:1] / channels
            row_var = both[:, 1:2] / channels - row_mean * row_mean
            normalized = (ng_ref[pl.ds(layer, 1), :] * (conv[span, :] - row_mean)
                          * lax.rsqrt(row_var + epsilon) + ns_ref[pl.ds(layer, 1), :])
            act_all[layer, span, mine] = jax.nn.silu(normalized).astype(jnp.bfloat16)

        def act_cols(who):
            return act_all.at[layer, :, pl.ds(pl.multiple_of(who * block, block), block)]

        partner = 2 * q + 1 - c
        copies = []
        for k in range(pairs - 1, -1, -1):
            target_t = 2 * ((q + k) % pairs) + c if k else partner
            copies.append(to_tp(act_cols(t), act_cols(t), asend.at[layer, k], arecv.at[layer, t], target_t))
            copies[-1].start()
        tend()
        for k in range(1, pairs):
            sender = 2 * ((q + k) % pairs) + c
            to_tp(act_cols(sender), act_cols(sender), asend.at[layer, k], arecv.at[layer, sender], sender).wait_recv()
            copies.append(to_tp(act_cols(sender), act_cols(sender), asend.at[layer, pairs + k],
                                arecv.at[layer, sender], partner))
            copies[-1].start()
        tend()
        ofull[layer, pl.ds(pl.multiple_of(t * block, block), block), :] = oring[
            layer, :, pl.ds(pl.multiple_of(c * half_width, half_width), half_width)]
        for k in range(1, m):
            peer = (t + k) % m

            @pl.loop(0, n)
            def _(piece, peer=peer):
                dst = ofull.at[layer, pl.ds(pl.multiple_of(peer * block, block), block),
                               pl.ds(pl.multiple_of(piece * ho, ho), ho)]
                to_tp(dst, dst, osend.at[layer, 0, 0, 0], orecv.at[layer, peer, piece], peer).wait_recv()

        for k in range(pairs):
            sender = 2 * ((q + k) % pairs) + 1 - c
            to_tp(act_cols(sender), act_cols(sender), asend.at[layer, k], arecv.at[layer, sender], partner).wait_recv()
        half = pl.ds(pl.multiple_of(c * half_width, half_width), half_width)
        branch = jnp.dot(act_all[layer], ofull[layer], preferred_element_type=jnp.float32).astype(jnp.bfloat16)
        target[:, half] = (source[:, half].astype(jnp.float32) + branch.astype(jnp.float32)).astype(jnp.bfloat16)
        swap = to_tp(target.at[:, half], target.at[:, half], xsend.at[layer], xrecv.at[layer], partner)
        swap.start()
        tend()
        swap.wait_recv()
        if nxt is not None:
            norm_rows(nxt, target)
        tend()
        for copy in copies + stat_copies + [halo_copy]:
            copy.wait_send()
        swap.wait_send()

    for layer in range(layers):
        layer_step(layer, tok_ref if layer == 0 else hid.at[layer - 1], hid.at[layer])
    out_ref[...] = hid[layers - 1]

    doc_copy.wait_send()

    @pl.loop(0, n - 1)
    def _(step):
        for layer in range(layers):
            for msg in range(3):
                for way in range(2):
                    ring_copy(layer, msg, way, step).wait_send()

    @pl.loop(0, n)
    def _(step):
        for layer in range(layers):
            for way in range(2):
                spread(layer, way, step, "wait_send")


def fused_on_device(n, m, tokens, doc_ids, pre_gain, value_proj, gate_proj, out_proj, conv_taps, norm_gain, norm_shift):
    rows, width = tokens.shape
    layers, depth, block = value_proj.shape
    owidth = out_proj.shape[2]
    reach = conv_taps.shape[1] - 1
    channels = block * m
    docs = doc_ids.reshape(rows // 128, 128)
    bf16, f32, i32 = jnp.bfloat16, jnp.float32, jnp.int32
    dma = pltpu.SemaphoreType.DMA
    vmem = pl.BlockSpec(memory_space=pltpu.VMEM)
    return pl.pallas_call(
        functools.partial(fused_kernel, n, m, reach, layers),
        out_shape=jax.ShapeDtypeStruct((rows, width), bf16),
        in_specs=[vmem] * 9,
        out_specs=vmem,
        scratch_shapes=[
            pltpu.VMEM((layers, n * depth, 2 * block), bf16),
            pltpu.VMEM((layers, block, n * owidth), bf16),
            pltpu.VMEM((layers, channels, width // 2), bf16),
            pltpu.VMEM((rows, width), bf16),
            pltpu.VMEM((rows, 2 * block), f32),
            pltpu.VMEM((block // 128 * (rows + HALO), 128), f32),
            pltpu.VMEM((rows + HALO, 128), f32),
            pltpu.VMEM((rows, 128), i32),
            pltpu.VMEM((layers, HALO, block), bf16),
            pltpu.VMEM((layers, HALO, block), bf16),
            pltpu.VMEM((HALO, 128), f32),
            pltpu.VMEM((HALO, 128), f32),
            pltpu.VMEM((rows, 128), f32),
            pltpu.VMEM((layers, 8, rows), f32),
            pltpu.VMEM((layers, m, 8, rows), f32),
            pltpu.VMEM((rows, block), f32),
            pltpu.VMEM((layers, rows, channels), bf16),
            pltpu.VMEM((layers, rows, width), bf16),
            dma((layers, 3, 2, n)), dma((layers, 3, 2, n)),
            dma((layers, 2, n, m // 2)), dma((layers, m, n)),
            dma((layers + 1,)), dma((layers + 1,)),
            dma((layers, m)), dma((layers, m)),
            dma((layers, m)), dma((layers, m)),
            dma((layers,)), dma((layers,)),
        ],
        compiler_params=pltpu.CompilerParams(
            collective_id=0, has_side_effects=True, vmem_limit_bytes=60 * 1024 * 1024),
    )(tokens, docs, pre_gain, value_proj, gate_proj, out_proj, jnp.transpose(conv_taps, (1, 0, 2)), norm_gain, norm_shift)


def passed_along(value, axis, steps):
    count = lax.axis_size(axis)
    first, last = (max(0, -steps), min(count, count - steps))
    return lax.ppermute(value, axis, [(source, source + steps) for source in range(first, last)])


def on_device(
    tokens, doc_ids, pre_gain, value_proj, gate_proj, out_proj, conv_taps, norm_gain, norm_shift
):
    layer_count = value_proj.shape[0]
    tap_count = conv_taps.shape[1]
    reach_rows = tap_count - 1
    row_count = tokens.shape[0]
    block_width = conv_taps.shape[2]
    channels = block_width * lax.axis_size("tp")
    hidden = tokens
    full_value, full_gate, full_out = (
        lax.all_gather(value_proj, "sp", axis=1, tiled=True),
        lax.all_gather(gate_proj, "sp", axis=1, tiled=True),
        lax.all_gather(out_proj, "sp", axis=2, tiled=True),
    )
    for layer_index in range(layer_count):
        wide_state = hidden.astype(jnp.float32)
        scale = lax.rsqrt(jnp.mean(wide_state * wide_state, axis=-1, keepdims=True) + epsilon)
        normed = (wide_state * scale * pre_gain[layer_index]).astype(jnp.bfloat16)
        value_acc = jnp.dot(normed, full_value[layer_index], preferred_element_type=jnp.float32)
        gate_acc = jnp.dot(normed, full_gate[layer_index], preferred_element_type=jnp.float32)
        value_half = value_acc.astype(jnp.bfloat16)
        gate_half = gate_acc.astype(jnp.bfloat16)
        gated_rows = (
            value_half.astype(jnp.float32) * jax.nn.sigmoid(gate_half.astype(jnp.float32))
        ).astype(jnp.bfloat16)
        prev_rows, prev_docs = passed_along(
            (gated_rows[row_count - reach_rows :], doc_ids[row_count - reach_rows :]), "sp", 1
        )
        padded = jnp.concatenate([prev_rows, gated_rows]).astype(jnp.float32)
        padded_docs = jnp.concatenate([prev_docs, doc_ids])
        conv_out = jnp.zeros((row_count, block_width), jnp.float32)
        for offset in range(tap_count):
            first_row = reach_rows - offset
            same_doc = (padded_docs[first_row : first_row + row_count] == doc_ids)[:, None]
            term = (
                conv_taps[layer_index, offset][None, :] * padded[first_row : first_row + row_count]
            )
            conv_out = conv_out + jnp.where(same_doc, term, jnp.float32(0.0))
        row_sums, square_sums = lax.psum(
            (jnp.sum(conv_out, axis=1), jnp.sum(conv_out * conv_out, axis=1)), "tp"
        )
        row_mean = (row_sums / channels)[:, None]
        row_var = (square_sums / channels)[:, None] - row_mean * row_mean
        normalized = (
            norm_gain[layer_index] * (conv_out - row_mean) * lax.rsqrt(row_var + epsilon)
            + norm_shift[layer_index]
        )
        activated = jax.nn.silu(normalized).astype(jnp.bfloat16)
        partial_value = jnp.dot(
            activated, full_out[layer_index], preferred_element_type=jnp.float32
        )
        summed = lax.psum(partial_value.astype(jnp.bfloat16), "tp")
        hidden = (hidden.astype(jnp.float32) + summed.astype(jnp.float32)).astype(jnp.bfloat16)
    return hidden


def suits_kernel(n, m, tokens, value_proj, out_proj, conv_taps):
    rows, width = tokens.shape
    depth, block = value_proj.shape[1:]
    return (
        n % 2 == 0 and 4 <= n <= 16 and m % 2 == 0 and m >= 4 and rows % 128 == 0 and width % 256 == 0
        and depth % 32 == 0 and block % 128 == 0 and out_proj.shape[2] % 256 == 0
        and conv_taps.shape[1] - 1 <= HALO
    )


def solution(mesh):
    n, m = mesh.shape["sp"], mesh.shape["tp"]

    def body(tokens, doc_ids, pre_gain, value_proj, gate_proj, out_proj, conv_taps, norm_gain, norm_shift):
        chosen = on_device
        if suits_kernel(n, m, tokens, value_proj, out_proj, conv_taps):
            chosen = functools.partial(fused_on_device, n, m)
        return chosen(tokens, doc_ids, pre_gain, value_proj, gate_proj, out_proj, conv_taps, norm_gain, norm_shift)

    return jax.shard_map(
        body,
        mesh=mesh,
        in_specs=(
            P("sp", None),
            P("sp"),
            P(),
            P(None, "sp", "tp"),
            P(None, "sp", "tp"),
            P(None, "tp", "sp"),
            P(None, None, "tp"),
            P(None, "tp"),
            P(None, "tp"),
        ),
        out_specs=P("sp", None),
        check_vma=False,
    )
```

profile of v0, /device:TPU:9, one launch (start us, length us, event | category | flops | bytes accessed | tf_op | source)
XLA Modules:
  0.0 98.0 jit_solution(14445615927979155627)
XLA Ops:
  0.0 95.2 %shard_map.91 = bf16[384,2048]{1,0:T(8,128)(2,1)} custom-call(bf16[384,2048]{1,0:T(8,128)(2,1)} %tok_ref.1, s32[3,128]{1,0:T(4,128)} %bitcast.3, f32[2,2048]{1,0:T(2,128)} %gain_ref.1, bf16[2,256,256]{2,1,0:T(8,128)(2,1)} %v_ref.1, bf16[2,256,256]{2,1,0:T(8,128)(2,1)} %g_ref.1, bf16[2,256,256]{2,1,0:T(8,128)(2,1)} %o_ref.1, f32[31,2,256]{2,1,0:T(2,128)} %bitcast.2, ...), custom_call_target="tpu_custom_call" | custom-call | tf_op jit(solution)/shard_map/pallas_call | solution.py:328
  95.2 2.7 %copy.11 = bf16[384,2048]{1,0:T(8,128)(2,1)} copy(bf16[384,2048]{1,0:T(8,128)(2,1)} %shard_map.91) | data formatting | bytes 3145728
where the time goes:
time: 99.9 us; the launch traced here: 98 us
  Pallas kernels  95.2 us (95%)
  local copies, waits for them, and re-layouts  2.73 us (3%)
    pallas_call x1, Pallas kernels, fused_on_device(): pl.pallas_call(functools.partial(fused_kernel, n, m, reach, layers), out_...  95.2 us
    unnamed x1, local copies, waits for them, and re-layouts  2.73 us

commit v1 on v0

v1 whole, which is shorter than its diff:
```python
import functools
import jax
import jax.numpy as jnp
from jax import lax
from jax.experimental import pallas as pl
from jax.experimental.pallas import tpu as pltpu
from jax.sharding import PartitionSpec as P

epsilon = 1e-06
MESH = pl.DeviceIdType.MESH
HALO = 32
CONV_ROWS = 64


def fused_kernel(
    n, m, reach, layers,
    tok_ref, doc_ref, gain_ref, v_ref, g_ref, o_ref, tap_ref, ng_ref, ns_ref,
    out_ref,
    w, oring, ofull, normed, acc, padded, pdoc, run, ghalo, halo_in, doc_in, doc_tail,
    stat, stat_out, stat_in, conv, act_all, hid,
    rsend, rrecv, osend, orecv, hsend, hrecv, ssend, srecv, asend, arecv, xsend, xrecv,
):
    me = lax.axis_index("sp")
    t = lax.axis_index("tp")
    q, c = t // 2, t % 2
    pairs = m // 2
    half_n = n // 2
    rows, width = tok_ref.shape
    depth, block = v_ref.shape[1], v_ref.shape[2]
    owidth = o_ref.shape[2]
    hb, ho = block // 2, owidth // 2
    half_width = width // 2
    channels = block * m

    def index_of(position):
        position = (position + 2 * n) % n
        return jnp.where(position < half_n, 2 * position, 2 * (n - 1 - position) + 1)

    my_pos = jnp.where(me % 2 == 0, me // 2, n - 1 - me // 2)
    right, left = index_of(my_pos + 1), index_of(my_pos - 1)
    following = (me + 1) % n

    barrier = pltpu.get_barrier_semaphore()
    for other in (right, left):
        pl.semaphore_signal(barrier, inc=1, device_id={"sp": other}, device_id_type=MESH)
    for k in range(1, m):
        pl.semaphore_signal(barrier, inc=1, device_id={"tp": (t + k) % m}, device_id_type=MESH)
    pl.semaphore_wait(barrier, 1 + m)

    def to_sp(src, dst, send, recv, target):
        return pltpu.make_async_remote_copy(
            src_ref=src, dst_ref=dst, send_sem=send, recv_sem=recv,
            device_id={"sp": target}, device_id_type=MESH)

    def to_tp(src, dst, send, recv, target):
        return pltpu.make_async_remote_copy(
            src_ref=src, dst_ref=dst, send_sem=send, recv_sem=recv,
            device_id={"tp": target}, device_id_type=MESH)

    def owner_at(way, distance):
        return index_of(my_pos - distance if way == 0 else my_pos + distance)

    def held(layer, kind, owner, piece):
        if kind < 2:
            return w.at[layer, kind, pl.ds(pl.multiple_of(owner * depth, depth), depth), pl.ds(piece * hb, hb)]
        return oring.at[layer, :, pl.ds(pl.multiple_of(owner * owidth + piece * ho, ho), ho)]

    def own_piece(layer, kind, piece):
        if kind < 2:
            return (v_ref, g_ref)[piece].at[layer, :, pl.ds(kind * hb, hb)]
        return o_ref.at[layer, :, pl.ds(piece * ho, ho)]

    def ring_copy(layer, kind, way, step, piece, src, dst):
        return to_sp(src, dst, rsend.at[layer, kind, way, step, piece], rrecv.at[layer, kind, way, step, piece],
                     right if way == 0 else left)

    def travels(way, step, piece):
        return step < half_n - 1 or piece == way

    def spread_copy(layer, way, step, piece, pair):
        owner = owner_at(way, step)
        part = owner // half_n
        local = owner - part * half_n
        src = own_piece(layer, 2, piece) if step == 0 else held(layer, 2, owner, piece)
        dst = ofull.at[layer, pl.ds(pl.multiple_of(t * block, block), block),
                       pl.ds(pl.multiple_of(local * owidth + piece * ho, ho), ho)]
        copy = to_tp(src, dst, osend.at[layer, way, step, piece, pair],
                     orecv.at[layer, t, local * 2 + piece], 2 * ((q + pair) % pairs) + part)
        return copy, part

    def spread(layer, way, step, piece, act):
        for pair in range(pairs - 1, -1, -1):
            copy, part = spread_copy(layer, way, step, piece, pair)
            if pair == 0:
                pl.when(part != c)(lambda copy=copy: getattr(copy, act)())
            else:
                getattr(copy, act)()

    def advance_one(layer, kind, step):
        for piece in range(2):
            for way in range(2):
                if step > 0:
                    if not travels(way, step - 1, piece):
                        continue
                    piece_ref = held(layer, kind, owner_at(way, step), piece)
                    ring_copy(layer, kind, way, step - 1, piece, piece_ref, piece_ref).wait_recv()
                if step < half_n and travels(way, step, piece):
                    dst = held(layer, kind, owner_at(way, step), piece)
                    src = own_piece(layer, kind, piece) if step == 0 else dst
                    ring_copy(layer, kind, way, step, piece, src, dst).start()
            if kind == 2:
                for way in range(2):
                    if step == 0 and way == 1 or step > 0 and not travels(way, step - 1, piece):
                        continue
                    spread(layer, way, step, piece, "start")

    entries = []
    for layer in range(layers):
        for step in range(half_n + 1):
            entries.append((11 * layer + 3.3 * step, layer, 0, step))
            entries.append((11 * layer + (2 if layer else 1) + 3.3 * step, layer, 1, step))
            entries.append((11 * layer + 5 + 3.2 * step, layer, 2, step))
    pending = [entry[1:] for entry in sorted(entries)]

    def tend(count):
        for _ in range(count):
            if pending:
                advance_one(*pending.pop(0))

    def advance(*target):
        while target in pending:
            advance_one(*pending.pop(0))

    def keep_own(layer):
        row = pl.ds(pl.multiple_of(me * depth, depth), depth)
        for kind in range(2):
            w[layer, kind, row, pl.ds(0, hb)] = v_ref[layer, :, kind * hb:(kind + 1) * hb]
            w[layer, kind, row, pl.ds(hb, hb)] = g_ref[layer, :, kind * hb:(kind + 1) * hb]
        oring[layer, :, pl.ds(pl.multiple_of(me * owidth, owidth), owidth)] = o_ref[layer]

    tend(2)

    def doc_block(i):
        row = doc_ref[pl.ds(i, 1), :].astype(jnp.float32)
        return jnp.transpose(jnp.broadcast_to(row, (128, 128)))

    doc_tail[...] = doc_block(rows // 128 - 1)[128 - HALO:]
    doc_copy = to_sp(doc_tail, doc_in, hsend.at[2 * layers], hrecv.at[2 * layers], following)

    for i in range(rows // 128):
        pdoc[pl.ds(HALO + i * 128, 128), :] = doc_block(i)
    pdoc[pl.ds(0, HALO), :] = jnp.full((HALO, 128), -1.0, jnp.float32)

    def norm_rows(layer, source):
        @pl.loop(0, rows // 32)
        def _(i):
            span = pl.ds(pl.multiple_of(i * 32, 32), 32)
            wide = source[span, :].astype(jnp.float32)
            scale = lax.rsqrt(jnp.mean(wide * wide, axis=-1, keepdims=True) + epsilon)
            normed[span, :] = (wide * scale * gain_ref[pl.ds(layer, 1), :]).astype(jnp.bfloat16)

    norm_rows(0, tok_ref)
    for layer in range(layers):
        keep_own(layer)

    @pl.when(me == 0)
    def _():
        halo_in[...] = jnp.zeros(halo_in.shape, halo_in.dtype)


    def count_runs():
        @pl.when(me > 0)
        def _():
            doc_copy.wait_recv()
            pdoc[pl.ds(0, HALO), :] = doc_in[...]

        @pl.loop(0, rows // CONV_ROWS)
        def _(i):
            base = pl.multiple_of(i * CONV_ROWS, CONV_ROWS)
            mine = pdoc[pl.ds(base + HALO, CONV_ROWS), :]
            count = jnp.zeros((CONV_ROWS, 128), jnp.int32)
            for j in range(1, reach + 1):
                count = count + (pdoc[pl.ds(base + (HALO - j), CONV_ROWS), :] == mine).astype(jnp.int32)
            run[pl.ds(base, CONV_ROWS), :] = count

    lane = lax.broadcasted_iota(jnp.int32, (CONV_ROWS, 128), 1)

    def layer_step(layer, source, target):
        last = layer + 1 == layers

        def halo_copy(kind):
            return to_sp(ghalo.at[layer, kind], halo_in.at[layer, kind],
                         hsend.at[2 * layer + kind], hrecv.at[2 * layer + kind], following)

        def store_padded(kind, row, values):
            padded[kind, pl.ds(row, 32), :] = values.astype(jnp.float32)

        def gate_half(kind):
            acc[...] = jnp.dot(normed[...], w[layer, kind], preferred_element_type=jnp.float32)

            def gate_rows(i):
                span = pl.ds(pl.multiple_of(i * 32, 32), 32)
                value = acc[span, pl.ds(0, hb)].astype(jnp.bfloat16).astype(jnp.float32)
                gate = acc[span, pl.ds(hb, hb)].astype(jnp.bfloat16).astype(jnp.float32)
                gated = (value * jax.nn.sigmoid(gate)).astype(jnp.bfloat16)
                store_padded(kind, pl.multiple_of(i * 32 + HALO, 32), gated)
                return gated

            ghalo[layer, kind] = gate_rows(rows // 32 - 1)
            pl.when(me < n - 1)(lambda: halo_copy(kind).start())

            @pl.loop(0, rows // 32 - 1)
            def _(i):
                gate_rows(i)

        def conv_half(kind):
            pl.when(me > 0)(lambda: halo_copy(kind).wait_recv())
            store_padded(kind, 0, halo_in[layer, kind])
            cols = pl.ds(kind * hb, hb)

            @pl.loop(0, rows // CONV_ROWS)
            def _(i):
                base = pl.multiple_of(i * CONV_ROWS, CONV_ROWS)
                count = run[pl.ds(base, CONV_ROWS), :]
                total = tap_ref[0, pl.ds(layer, 1), cols] * padded[kind, pl.ds(base + HALO, CONV_ROWS), :]
                for j in range(1, reach + 1):
                    term = tap_ref[j, pl.ds(layer, 1), cols] * padded[kind, pl.ds(base + (HALO - j), CONV_ROWS), :]
                    total = total + jnp.where(count >= j, term, jnp.float32(0.0))
                conv[pl.ds(base, CONV_ROWS), cols] = total
                sums = jnp.where(
                    lane == 0, jnp.sum(total, axis=1, keepdims=True),
                    jnp.where(lane == 1, jnp.sum(total * total, axis=1, keepdims=True), jnp.float32(0.0)))
                if kind:
                    sums = sums + stat[pl.ds(base, CONV_ROWS), :]
                stat[pl.ds(base, CONV_ROWS), :] = sums

        advance(layer, 0, half_n)
        if layer == 0:
            pl.when(me < n - 1)(doc_copy.start)
        gate_half(0)
        if last:
            tend(1)
            conv_half(0)
        advance(layer, 1, half_n)
        gate_half(1)
        if layer == 0:
            count_runs()
        if last:
            advance(layer, 2, half_n)
        else:
            tend(1)
            conv_half(0)
            tend(1)
        conv_half(1)

        stat_out[layer] = jnp.transpose(stat[...])[:8]
        stat_copies = [
            to_tp(stat_out.at[layer], stat_in.at[layer, t], ssend.at[layer, k], srecv.at[layer, t], (t + k) % m)
            for k in range(1, m)]
        for copy in stat_copies:
            copy.start()
        if not last:
            tend(1)
        summed = stat_out[layer]
        for k in range(1, m):
            peer = (t + k) % m
            to_tp(stat_in.at[layer, peer], stat_in.at[layer, peer], ssend.at[layer, k],
                  srecv.at[layer, peer], peer).wait_recv()
            summed = summed + stat_in[layer, peer]
        stat[...] = jnp.transpose(
            jnp.concatenate([summed, jnp.zeros((120, rows), jnp.float32)], axis=0))

        mine = pl.ds(pl.multiple_of(t * block, block), block)

        @pl.loop(0, rows // CONV_ROWS)
        def _(i):
            span = pl.ds(pl.multiple_of(i * CONV_ROWS, CONV_ROWS), CONV_ROWS)
            both = stat[span, :]
            row_mean = both[:, 0:1] / channels
            row_var = both[:, 1:2] / channels - row_mean * row_mean
            normalized = (ng_ref[pl.ds(layer, 1), :] * (conv[span, :] - row_mean)
                          * lax.rsqrt(row_var + epsilon) + ns_ref[pl.ds(layer, 1), :])
            act_all[layer, span, mine] = jax.nn.silu(normalized).astype(jnp.bfloat16)

        def act_cols(who):
            return act_all.at[layer, :, pl.ds(pl.multiple_of(who * block, block), block)]

        partner = 2 * q + 1 - c
        copies = []
        for k in range(pairs - 1, -1, -1):
            target_t = 2 * ((q + k) % pairs) + c if k else partner
            copies.append(to_tp(act_cols(t), act_cols(t), asend.at[layer, k], arecv.at[layer, t], target_t))
            copies[-1].start()
        if not last:
            tend(2)
        for k in range(1, pairs):
            sender = 2 * ((q + k) % pairs) + c
            to_tp(act_cols(sender), act_cols(sender), asend.at[layer, k], arecv.at[layer, sender], sender).wait_recv()
            copies.append(to_tp(act_cols(sender), act_cols(sender), asend.at[layer, pairs + k],
                                arecv.at[layer, sender], partner))
            copies[-1].start()
        if not last:
            advance(layer, 2, half_n)
            tend(1)
        ofull[layer, pl.ds(pl.multiple_of(t * block, block), block), :] = oring[
            layer, :, pl.ds(pl.multiple_of(c * half_width, half_width), half_width)]
        for k in range(1, m):
            peer = (t + k) % m

            @pl.loop(0, n)
            def _(piece, peer=peer):
                dst = ofull.at[layer, pl.ds(pl.multiple_of(peer * block, block), block),
                               pl.ds(pl.multiple_of(piece * ho, ho), ho)]
                to_tp(dst, dst, osend.at[layer, 0, 0, 0, 0], orecv.at[layer, peer, piece], peer).wait_recv()

        for k in range(pairs):
            sender = 2 * ((q + k) % pairs) + 1 - c
            to_tp(act_cols(sender), act_cols(sender), asend.at[layer, k], arecv.at[layer, sender], partner).wait_recv()
        half = pl.ds(pl.multiple_of(c * half_width, half_width), half_width)
        branch = jnp.dot(act_all[layer], ofull[layer], preferred_element_type=jnp.float32).astype(jnp.bfloat16)
        target[:, half] = (source[:, half].astype(jnp.float32) + branch.astype(jnp.float32)).astype(jnp.bfloat16)
        swap = to_tp(target.at[:, half], target.at[:, half], xsend.at[layer], xrecv.at[layer], partner)
        swap.start()
        if not last:
            tend(1)
        swap.wait_recv()
        if not last:
            norm_rows(layer + 1, target)
            tend(1)
        for copy in copies + stat_copies:
            copy.wait_send()
        for kind in range(2):
            pl.when(me < n - 1)(lambda kind=kind: halo_copy(kind).wait_send())
        swap.wait_send()

    for layer in range(layers):
        layer_step(layer, tok_ref if layer == 0 else hid.at[layer - 1], hid.at[layer])
    out_ref[...] = hid[layers - 1]

    pl.when(me < n - 1)(doc_copy.wait_send)

    for layer in range(layers):
        for way in range(2):
            for piece in range(2):
                for kind in range(3):
                    @pl.loop(0, half_n if piece == way else half_n - 1)
                    def _(step, layer=layer, way=way, piece=piece, kind=kind):
                        ref = held(layer, kind, me, piece)
                        ring_copy(layer, kind, way, step, piece, ref, ref).wait_send()

                @pl.loop(1 if way else 0, half_n + 1 if piece == way else half_n)
                def _(step, layer=layer, way=way, piece=piece):
                    for pair in range(pairs):
                        part = owner_at(way, step) // half_n
                        ref = held(layer, 2, me, piece)
                        copy = to_tp(ref, ref, osend.at[layer, way, step, piece, pair],
                                     orecv.at[layer, t, 0], 2 * ((q + pair) % pairs) + part)
                        if pair == 0:
                            pl.when(part != c)(copy.wait_send)
                        else:
                            copy.wait_send()


def fused_on_device(n, m, tokens, doc_ids, pre_gain, value_proj, gate_proj, out_proj, conv_taps, norm_gain, norm_shift):
    rows, width = tokens.shape
    layers, depth, block = value_proj.shape
    owidth = out_proj.shape[2]
    reach = conv_taps.shape[1] - 1
    channels = block * m
    docs = doc_ids.reshape(rows // 128, 128)
    bf16, f32, i32 = jnp.bfloat16, jnp.float32, jnp.int32
    dma = pltpu.SemaphoreType.DMA
    vmem = pl.BlockSpec(memory_space=pltpu.VMEM)
    return pl.pallas_call(
        functools.partial(fused_kernel, n, m, reach, layers),
        out_shape=jax.ShapeDtypeStruct((rows, width), bf16),
        in_specs=[vmem] * 9,
        out_specs=vmem,
        scratch_shapes=[
            pltpu.VMEM((layers, 2, n * depth, block), bf16),
            pltpu.VMEM((layers, block, n * owidth), bf16),
            pltpu.VMEM((layers, channels, width // 2), bf16),
            pltpu.VMEM((rows, width), bf16),
            pltpu.VMEM((rows, block), f32),
            pltpu.VMEM((2, rows + HALO, block // 2), f32),
            pltpu.VMEM((rows + HALO, 128), f32),
            pltpu.VMEM((rows, 128), i32),
            pltpu.VMEM((layers, 2, HALO, block // 2), bf16),
            pltpu.VMEM((layers, 2, HALO, block // 2), bf16),
            pltpu.VMEM((HALO, 128), f32),
            pltpu.VMEM((HALO, 128), f32),
            pltpu.VMEM((rows, 128), f32),
            pltpu.VMEM((layers, 8, rows), f32),
            pltpu.VMEM((layers, m, 8, rows), f32),
            pltpu.VMEM((rows, block), f32),
            pltpu.VMEM((layers, rows, channels), bf16),
            pltpu.VMEM((layers, rows, width), bf16),
            dma((layers, 3, 2, n // 2, 2)), dma((layers, 3, 2, n // 2, 2)),
            dma((layers, 2, n // 2 + 1, 2, m // 2)), dma((layers, m, n)),
            dma((2 * layers + 1,)), dma((2 * layers + 1,)),
            dma((layers, m)), dma((layers, m)),
            dma((layers, m)), dma((layers, m)),
            dma((layers,)), dma((layers,)),
        ],
        compiler_params=pltpu.CompilerParams(
            collective_id=0, has_side_effects=True, vmem_limit_bytes=60 * 1024 * 1024),
    )(tokens, docs, pre_gain, value_proj, gate_proj, out_proj, jnp.transpose(conv_taps, (1, 0, 2)), norm_gain, norm_shift)


def passed_along(value, axis, steps):
    count = lax.axis_size(axis)
    first, last = (max(0, -steps), min(count, count - steps))
    return lax.ppermute(value, axis, [(source, source + steps) for source in range(first, last)])


def on_device(
    tokens, doc_ids, pre_gain, value_proj, gate_proj, out_proj, conv_taps, norm_gain, norm_shift
):
    layer_count = value_proj.shape[0]
    tap_count = conv_taps.shape[1]
    reach_rows = tap_count - 1
    row_count = tokens.shape[0]
    block_width = conv_taps.shape[2]
    channels = block_width * lax.axis_size("tp")
    hidden = tokens
    full_value, full_gate, full_out = (
        lax.all_gather(value_proj, "sp", axis=1, tiled=True),
        lax.all_gather(gate_proj, "sp", axis=1, tiled=True),
        lax.all_gather(out_proj, "sp", axis=2, tiled=True),
    )
    for layer_index in range(layer_count):
        wide_state = hidden.astype(jnp.float32)
        scale = lax.rsqrt(jnp.mean(wide_state * wide_state, axis=-1, keepdims=True) + epsilon)
        normed = (wide_state * scale * pre_gain[layer_index]).astype(jnp.bfloat16)
        value_acc = jnp.dot(normed, full_value[layer_index], preferred_element_type=jnp.float32)
        gate_acc = jnp.dot(normed, full_gate[layer_index], preferred_element_type=jnp.float32)
        value_half = value_acc.astype(jnp.bfloat16)
        gate_half = gate_acc.astype(jnp.bfloat16)
        gated_rows = (
            value_half.astype(jnp.float32) * jax.nn.sigmoid(gate_half.astype(jnp.float32))
        ).astype(jnp.bfloat16)
        prev_rows, prev_docs = passed_along(
            (gated_rows[row_count - reach_rows :], doc_ids[row_count - reach_rows :]), "sp", 1
        )
        padded = jnp.concatenate([prev_rows, gated_rows]).astype(jnp.float32)
        padded_docs = jnp.concatenate([prev_docs, doc_ids])
        conv_out = jnp.zeros((row_count, block_width), jnp.float32)
        for offset in range(tap_count):
            first_row = reach_rows - offset
            same_doc = (padded_docs[first_row : first_row + row_count] == doc_ids)[:, None]
            term = (
                conv_taps[layer_index, offset][None, :] * padded[first_row : first_row + row_count]
            )
            conv_out = conv_out + jnp.where(same_doc, term, jnp.float32(0.0))
        row_sums, square_sums = lax.psum(
            (jnp.sum(conv_out, axis=1), jnp.sum(conv_out * conv_out, axis=1)), "tp"
        )
        row_mean = (row_sums / channels)[:, None]
        row_var = (square_sums / channels)[:, None] - row_mean * row_mean
        normalized = (
            norm_gain[layer_index] * (conv_out - row_mean) * lax.rsqrt(row_var + epsilon)
            + norm_shift[layer_index]
        )
        activated = jax.nn.silu(normalized).astype(jnp.bfloat16)
        partial_value = jnp.dot(
            activated, full_out[layer_index], preferred_element_type=jnp.float32
        )
        summed = lax.psum(partial_value.astype(jnp.bfloat16), "tp")
        hidden = (hidden.astype(jnp.float32) + summed.astype(jnp.float32)).astype(jnp.bfloat16)
    return hidden


def suits_kernel(n, m, tokens, value_proj, out_proj, conv_taps):
    rows, width = tokens.shape
    depth, block = value_proj.shape[1:]
    return (
        n % 2 == 0 and 4 <= n <= 16 and m % 2 == 0 and m >= 4 and rows % 128 == 0 and width % 256 == 0
        and depth % 32 == 0 and block == 256 and out_proj.shape[2] % 256 == 0
        and conv_taps.shape[1] - 1 <= HALO
    )


def solution(mesh):
    n, m = mesh.shape["sp"], mesh.shape["tp"]

    def body(tokens, doc_ids, pre_gain, value_proj, gate_proj, out_proj, conv_taps, norm_gain, norm_shift):
        chosen = on_device
        if suits_kernel(n, m, tokens, value_proj, out_proj, conv_taps):
            chosen = functools.partial(fused_on_device, n, m)
        return chosen(tokens, doc_ids, pre_gain, value_proj, gate_proj, out_proj, conv_taps, norm_gain, norm_shift)

    return jax.shard_map(
        body,
        mesh=mesh,
        in_specs=(
            P("sp", None),
            P("sp"),
            P(),
            P(None, "sp", "tp"),
            P(None, "sp", "tp"),
            P(None, "tp", "sp"),
            P(None, None, "tp"),
            P(None, "tp"),
            P(None, "tp"),
        ),
        out_specs=P("sp", None),
        check_vma=False,
    )
```

time: 99.9 us -> 104 us (1.041); the launches traced: 98 us -> 104 us
  Pallas kernels: 95.2 us -> 101 us
    pallas_call x1, Pallas kernels: 95.2 us -> 101 us  [fused_on_device(): pl.pallas_call(functools.partial(fused_kernel, n, m, reach, layers), out_...]
where the time goes in v1:
time: 104 us
  Pallas kernels  101 us (97%)
  local copies, waits for them, and re-layouts  2.73 us (3%)
    pallas_call x1, Pallas kernels, fused_on_device(): pl.pallas_call(functools.partial(fused_kernel, n, m, reach, layers), out_...  101 us
    unnamed x1, local copies, waits for them, and re-layouts  2.73 us

profile of v1, /device:TPU:9, one launch (start us, length us, event | category | flops | bytes accessed | tf_op | source)
XLA Modules:
  0.0 104.2 jit_solution(9257235482582880696)
XLA Ops:
  0.0 101.5 %shard_map.91 = bf16[384,2048]{1,0:T(8,128)(2,1)} custom-call(bf16[384,2048]{1,0:T(8,128)(2,1)} %tok_ref.1, s32[3,128]{1,0:T(4,128)} %bitcast.3, f32[2,2048]{1,0:T(2,128)} %gain_ref.1, bf16[2,256,256]{2,1,0:T(8,128)(2,1)} %v_ref.1, bf16[2,256,256]{2,1,0:T(8,128)(2,1)} %g_ref.1, bf16[2,256,256]{2,1,0:T(8,128)(2,1)} %o_ref.1, f32[31,2,256]{2,1,0:T(2,128)} %bitcast.2, ...), custom_call_target="tpu_custom_call" | custom-call | tf_op jit(solution)/shard_map/pallas_call | solution.py:374
  101.5 2.7 %copy.11 = bf16[384,2048]{1,0:T(8,128)(2,1)} copy(bf16[384,2048]{1,0:T(8,128)(2,1)} %shard_map.91) | data formatting | bytes 3145728

commit v2 on v1

--- a/solution.py
+++ b/solution.py
@@ -16,9 +16,9 @@
     n, m, reach, layers,
     tok_ref, doc_ref, gain_ref, v_ref, g_ref, o_ref, tap_ref, ng_ref, ns_ref,
     out_ref,
-    w, oring, ofull, normed, acc, padded, pdoc, run, ghalo, halo_in, doc_in, doc_tail,
-    stat, stat_out, stat_in, conv, act_all, hid,
-    rsend, rrecv, osend, orecv, hsend, hrecv, ssend, srecv, asend, arecv, xsend, xrecv,
+    w, oall, normed, acc, padded, pdoc, run, ghalo, halo_in, doc_in, doc_tail,
+    stat, stats, ng_all, ns_all, conv, act, psend, precv, hid,
+    rsend, rrecv, osend, orecv, hsend, hrecv, ssend, srecv, csend, crecv, xsend, xrecv, gsend, grecv, wsem,
 ):
     me = lax.axis_index("sp")
     t = lax.axis_index("tp")
@@ -29,7 +29,6 @@
     depth, block = v_ref.shape[1], v_ref.shape[2]
     owidth = o_ref.shape[2]
     hb, ho = block // 2, owidth // 2
-    half_width = width // 2
     channels = block * m
 
     def index_of(position):
@@ -63,7 +62,8 @@
     def held(layer, kind, owner, piece):
         if kind < 2:
             return w.at[layer, kind, pl.ds(pl.multiple_of(owner * depth, depth), depth), pl.ds(piece * hb, hb)]
-        return oring.at[layer, :, pl.ds(pl.multiple_of(owner * owidth + piece * ho, ho), ho)]
+        return oall.at[layer, pl.ds(pl.multiple_of(q * block, block), block),
+                       pl.ds(pl.multiple_of(owner * owidth + piece * ho, ho), ho)]
 
     def own_piece(layer, kind, piece):
         if kind < 2:
@@ -77,41 +77,28 @@
     def travels(way, step, piece):
         return step < half_n - 1 or piece == way
 
-    def spread_copy(layer, way, step, piece, pair):
+    def spread(layer, way, step, piece, act):
         owner = owner_at(way, step)
-        part = owner // half_n
-        local = owner - part * half_n
-        src = own_piece(layer, 2, piece) if step == 0 else held(layer, 2, owner, piece)
-        dst = ofull.at[layer, pl.ds(pl.multiple_of(t * block, block), block),
-                       pl.ds(pl.multiple_of(local * owidth + piece * ho, ho), ho)]
-        copy = to_tp(src, dst, osend.at[layer, way, step, piece, pair],
-                     orecv.at[layer, t, local * 2 + piece], 2 * ((q + pair) % pairs) + part)
-        return copy, part
-
-    def spread(layer, way, step, piece, act):
-        for pair in range(pairs - 1, -1, -1):
-            copy, part = spread_copy(layer, way, step, piece, pair)
-            if pair == 0:
-                pl.when(part != c)(lambda copy=copy: getattr(copy, act)())
-            else:
-                getattr(copy, act)()
+        part = held(layer, 2, owner, piece)
+        src = own_piece(layer, 2, piece) if step == 0 else part
+        for k in range(1, pairs):
+            copy = to_tp(src, part, osend.at[layer, way, step, piece, k - 1],
+                         orecv.at[layer, q, owner * 2 + piece], 2 * ((q + k) % pairs) + c)
+            getattr(copy, act)()
 
     def advance_one(layer, kind, step):
-        for piece in range(2):
+        for turn in range(2):
             for way in range(2):
-                if step > 0:
-                    if not travels(way, step - 1, piece):
-                        continue
+                piece = turn ^ way
+                arrived = step == 0 or travels(way, step - 1, piece)
+                if step > 0 and arrived:
                     piece_ref = held(layer, kind, owner_at(way, step), piece)
                     ring_copy(layer, kind, way, step - 1, piece, piece_ref, piece_ref).wait_recv()
                 if step < half_n and travels(way, step, piece):
                     dst = held(layer, kind, owner_at(way, step), piece)
                     src = own_piece(layer, kind, piece) if step == 0 else dst
                     ring_copy(layer, kind, way, step, piece, src, dst).start()
-            if kind == 2:
-                for way in range(2):
-                    if step == 0 and way == 1 or step > 0 and not travels(way, step - 1, piece):
-                        continue
+                if kind == 2 and arrived and (step > 0 or way == 0):
                     spread(layer, way, step, piece, "start")
 
     entries = []
@@ -119,7 +106,7 @@
         for step in range(half_n + 1):
             entries.append((11 * layer + 3.3 * step, layer, 0, step))
             entries.append((11 * layer + (2 if layer else 1) + 3.3 * step, layer, 1, step))
-            entries.append((11 * layer + 5 + 3.2 * step, layer, 2, step))
+            entries.append((11 * layer + (2.5 if layer else 5) + 3.2 * step, layer, 2, step))
     pending = [entry[1:] for entry in sorted(entries)]
 
     def tend(count):
@@ -136,9 +123,18 @@
         for kind in range(2):
             w[layer, kind, row, pl.ds(0, hb)] = v_ref[layer, :, kind * hb:(kind + 1) * hb]
             w[layer, kind, row, pl.ds(hb, hb)] = g_ref[layer, :, kind * hb:(kind + 1) * hb]
-        oring[layer, :, pl.ds(pl.multiple_of(me * owidth, owidth), owidth)] = o_ref[layer]
+        oall[layer, pl.ds(pl.multiple_of(q * block, block), block),
+             pl.ds(pl.multiple_of(me * owidth, owidth), owidth)] = o_ref[layer]
 
     tend(2)
+    gain_copies = []
+    for k in range(1, pairs):
+        for index, (src, dst) in enumerate(((ng_ref, ng_all), (ns_ref, ns_all))):
+            copy = to_tp(src, dst.at[q], gsend.at[k, index], grecv.at[q, index], 2 * ((q + k) % pairs) + c)
+            copy.start()
+            gain_copies.append(copy)
+    ng_all[q] = ng_ref[...]
+    ns_all[q] = ns_ref[...]
 
     def doc_block(i):
         row = doc_ref[pl.ds(i, 1), :].astype(jnp.float32)
@@ -169,6 +165,11 @@
 
 
     def count_runs():
+        for k in range(1, pairs):
+            for index, dst in enumerate((ng_all, ns_all)):
+                peer = (q + k) % pairs
+                to_tp(dst.at[peer], dst.at[peer], gsend.at[k, index], grecv.at[peer, index], t).wait_recv()
+
         @pl.when(me > 0)
         def _():
             doc_copy.wait_recv()
@@ -184,9 +185,17 @@
             run[pl.ds(base, CONV_ROWS), :] = count
 
     lane = lax.broadcasted_iota(jnp.int32, (CONV_ROWS, 128), 1)
+    chunks = rows // 128
+    order = list(range(1, chunks)) + [0]
+    partner = 2 * q + 1 - c
 
     def layer_step(layer, source, target):
         last = layer + 1 == layers
+        marks = [1, 1, 1, 1, 1, 1, 1, 1, 1]
+
+        def pause():
+            if not last and marks:
+                tend(marks.pop(0))
 
         def halo_copy(kind):
             return to_sp(ghalo.at[layer, kind], halo_in.at[layer, kind],
@@ -213,26 +222,54 @@
             def _(i):
                 gate_rows(i)
 
-        def conv_half(kind):
+        def take_halo(kind):
             pl.when(me > 0)(lambda: halo_copy(kind).wait_recv())
             store_padded(kind, 0, halo_in[layer, kind])
+
+        def conv_rows(kind, first, end):
             cols = pl.ds(kind * hb, hb)
 
-            @pl.loop(0, rows // CONV_ROWS)
+            @pl.loop(first, end)
             def _(i):
                 base = pl.multiple_of(i * CONV_ROWS, CONV_ROWS)
-                count = run[pl.ds(base, CONV_ROWS), :]
+                span = pl.ds(base, CONV_ROWS)
+                count = run[span, :]
                 total = tap_ref[0, pl.ds(layer, 1), cols] * padded[kind, pl.ds(base + HALO, CONV_ROWS), :]
                 for j in range(1, reach + 1):
                     term = tap_ref[j, pl.ds(layer, 1), cols] * padded[kind, pl.ds(base + (HALO - j), CONV_ROWS), :]
                     total = total + jnp.where(count >= j, term, jnp.float32(0.0))
-                conv[pl.ds(base, CONV_ROWS), cols] = total
+                conv[layer, q, span, cols] = total.astype(jnp.bfloat16)
                 sums = jnp.where(
                     lane == 0, jnp.sum(total, axis=1, keepdims=True),
                     jnp.where(lane == 1, jnp.sum(total * total, axis=1, keepdims=True), jnp.float32(0.0)))
                 if kind:
-                    sums = sums + stat[pl.ds(base, CONV_ROWS), :]
-                stat[pl.ds(base, CONV_ROWS), :] = sums
+                    sums = sums + stat[span, :]
+                stat[span, :] = sums
+
+        def conv_copies(kind, chunk, p, act):
+            span = pl.ds(chunk * 128, 128) if kind else pl.ds(0, rows)
+            slot = chunk + 1 if kind else 0
+            for k in range(1, pairs):
+                peer = (q + k) % pairs
+                part = conv.at[layer, p if p is not None else peer, span, pl.ds(kind * hb, hb)]
+                copy = to_tp(part, part, csend.at[layer, k, slot],
+                             crecv.at[layer, p if p is not None else peer, slot], 2 * peer + c)
+                getattr(copy, act)()
+
+        def stat_copy(chunk, k, who):
+            part = stats.at[layer, who, chunk]
+            return to_tp(part, part, ssend.at[layer, k, chunk], srecv.at[layer, who, chunk], (t + k) % m)
+
+        def swap_copy(chunk):
+            span = pl.ds(chunk * 128, 128)
+            return to_tp(psend.at[layer, span], precv.at[layer, span], xsend.at[layer, chunk],
+                         xrecv.at[layer, chunk], partner)
+
+        def first_half():
+            conv_rows(0, 1, rows // CONV_ROWS)
+            take_halo(0)
+            conv_rows(0, 0, 1)
+            conv_copies(0, 0, q, "start")
 
         advance(layer, 0, half_n)
         if layer == 0:
@@ -240,102 +277,97 @@
         gate_half(0)
         if last:
             tend(1)
-            conv_half(0)
+            first_half()
         advance(layer, 1, half_n)
         gate_half(1)
-        if layer == 0:
-            count_runs()
         if last:
             advance(layer, 2, half_n)
         else:
-            tend(1)
-            conv_half(0)
-            tend(1)
-        conv_half(1)
-
-        stat_out[layer] = jnp.transpose(stat[...])[:8]
-        stat_copies = [
-            to_tp(stat_out.at[layer], stat_in.at[layer, t], ssend.at[layer, k], srecv.at[layer, t], (t + k) % m)
-            for k in range(1, m)]
-        for copy in stat_copies:
-            copy.start()
-        if not last:
-            tend(1)
-        summed = stat_out[layer]
-        for k in range(1, m):
-            peer = (t + k) % m
-            to_tp(stat_in.at[layer, peer], stat_in.at[layer, peer], ssend.at[layer, k],
-                  srecv.at[layer, peer], peer).wait_recv()
-            summed = summed + stat_in[layer, peer]
-        stat[...] = jnp.transpose(
-            jnp.concatenate([summed, jnp.zeros((120, rows), jnp.float32)], axis=0))
-
-        mine = pl.ds(pl.multiple_of(t * block, block), block)
-
-        @pl.loop(0, rows // CONV_ROWS)
-        def _(i):
-            span = pl.ds(pl.multiple_of(i * CONV_ROWS, CONV_ROWS), CONV_ROWS)
-            both = stat[span, :]
+            if layer == 0:
+                count_runs()
+            pause()
+            first_half()
+        for chunk in order:
+            if chunk == 0:
+                pause()
+                take_halo(1)
+            conv_rows(1, 2 * chunk, 2 * chunk + 2)
+            stats[layer, t, chunk] = jnp.transpose(stat[pl.ds(chunk * 128, 128), :])[:8]
+            for k in range(1, m):
+                stat_copy(chunk, k, t).start()
+            conv_copies(1, chunk, q, "start")
+
+        pause()
+        pause()
+        gains = [ng_all[p, pl.ds(layer, 1), :] for p in range(pairs)]
+        shifts = [ns_all[p, pl.ds(layer, 1), :] for p in range(pairs)]
+        for chunk in order:
+            for k in range(1, m):
+                stat_copy(chunk, k, (t + k) % m).wait_recv()
+            summed = stats[layer, 0, chunk]
+            for who in range(1, m):
+                summed = summed + stats[layer, who, chunk]
+            both = jnp.transpose(jnp.concatenate([summed, jnp.zeros((120, 128), jnp.float32)], axis=0))
             row_mean = both[:, 0:1] / channels
             row_var = both[:, 1:2] / channels - row_mean * row_mean
-            normalized = (ng_ref[pl.ds(layer, 1), :] * (conv[span, :] - row_mean)
-                          * lax.rsqrt(row_var + epsilon) + ns_ref[pl.ds(layer, 1), :])
-            act_all[layer, span, mine] = jax.nn.silu(normalized).astype(jnp.bfloat16)
-
-        def act_cols(who):
-            return act_all.at[layer, :, pl.ds(pl.multiple_of(who * block, block), block)]
-
-        partner = 2 * q + 1 - c
-        copies = []
-        for k in range(pairs - 1, -1, -1):
-            target_t = 2 * ((q + k) % pairs) + c if k else partner
-            copies.append(to_tp(act_cols(t), act_cols(t), asend.at[layer, k], arecv.at[layer, t], target_t))
-            copies[-1].start()
-        if not last:
-            tend(2)
-        for k in range(1, pairs):
-            sender = 2 * ((q + k) % pairs) + c
-            to_tp(act_cols(sender), act_cols(sender), asend.at[layer, k], arecv.at[layer, sender], sender).wait_recv()
-            copies.append(to_tp(act_cols(sender), act_cols(sender), asend.at[layer, pairs + k],
-                                arecv.at[layer, sender], partner))
-            copies[-1].start()
-        if not last:
-            advance(layer, 2, half_n)
-            tend(1)
-        ofull[layer, pl.ds(pl.multiple_of(t * block, block), block), :] = oring[
-            layer, :, pl.ds(pl.multiple_of(c * half_width, half_width), half_width)]
-        for k in range(1, m):
-            peer = (t + k) % m
-
-            @pl.loop(0, n)
-            def _(piece, peer=peer):
-                dst = ofull.at[layer, pl.ds(pl.multiple_of(peer * block, block), block),
-                               pl.ds(pl.multiple_of(piece * ho, ho), ho)]
-                to_tp(dst, dst, osend.at[layer, 0, 0, 0, 0], orecv.at[layer, peer, piece], peer).wait_recv()
-
-        for k in range(pairs):
-            sender = 2 * ((q + k) % pairs) + 1 - c
-            to_tp(act_cols(sender), act_cols(sender), asend.at[layer, k], arecv.at[layer, sender], partner).wait_recv()
-        half = pl.ds(pl.multiple_of(c * half_width, half_width), half_width)
-        branch = jnp.dot(act_all[layer], ofull[layer], preferred_element_type=jnp.float32).astype(jnp.bfloat16)
-        target[:, half] = (source[:, half].astype(jnp.float32) + branch.astype(jnp.float32)).astype(jnp.bfloat16)
-        swap = to_tp(target.at[:, half], target.at[:, half], xsend.at[layer], xrecv.at[layer], partner)
-        swap.start()
-        if not last:
-            tend(1)
-        swap.wait_recv()
-        if not last:
-            norm_rows(layer + 1, target)
-            tend(1)
-        for copy in copies + stat_copies:
-            copy.wait_send()
+            row_scale = lax.rsqrt(row_var + epsilon)
+            if chunk == order[0]:
+                conv_copies(0, 0, None, "wait_recv")
+            conv_copies(1, chunk, None, "wait_recv")
+            span = pl.ds(chunk * 128, 128)
+            for p in range(pairs):
+                normalized = gains[p] * (conv[layer, p, span, :].astype(jnp.float32) - row_mean) * row_scale + shifts[p]
+                act[span, pl.ds(p * block, block)] = jax.nn.silu(normalized).astype(jnp.bfloat16)
+            if chunk == order[0]:
+                if not last:
+                    pause()
+                    advance(layer, 2, half_n)
+                for k in range(1, pairs):
+                    peer = (q + k) % pairs
+
+                    @pl.loop(0, 2 * n)
+                    def _(piece, peer=peer):
+                        part = oall.at[layer, pl.ds(pl.multiple_of(peer * block, block), block),
+                                       pl.ds(pl.multiple_of(piece * ho, ho), ho)]
+                        to_tp(part, part, osend.at[layer, 0, 0, 0, 0], orecv.at[layer, peer, piece], t).wait_recv()
+            psend[layer, span, :] = jnp.dot(
+                act[span, :], oall[layer], preferred_element_type=jnp.float32).astype(jnp.bfloat16)
+            swap_copy(chunk).start()
+            pause()
+
+        for chunk in order:
+            swap_copy(chunk).wait_recv()
+
+            @pl.loop(0, 128 // 32)
+            def _(i, chunk=chunk):
+                span = pl.ds(pl.multiple_of(chunk * 128 + i * 32, 32), 32)
+                branch = (psend[layer, span, :].astype(jnp.float32)
+                          + precv[layer, span, :].astype(jnp.float32)).astype(jnp.bfloat16)
+                total = (source[span, :].astype(jnp.float32) + branch.astype(jnp.float32)).astype(jnp.bfloat16)
+                target[span, :] = total
+                if not last:
+                    wide = total.astype(jnp.float32)
+                    scale = lax.rsqrt(jnp.mean(wide * wide, axis=-1, keepdims=True) + epsilon)
+                    normed[span, :] = (wide * scale * gain_ref[pl.ds(layer + 1, 1), :]).astype(jnp.bfloat16)
+
+            if last:
+                span = pl.ds(chunk * 128, 128)
+                pltpu.make_async_copy(target.at[span], out_ref.at[span], wsem.at[chunk]).start()
+            pause()
+
+        for chunk in range(chunks):
+            for k in range(1, m):
+                stat_copy(chunk, k, t).wait_send()
+            conv_copies(1, chunk, q, "wait_send")
+            swap_copy(chunk).wait_send()
+        conv_copies(0, 0, q, "wait_send")
         for kind in range(2):
             pl.when(me < n - 1)(lambda kind=kind: halo_copy(kind).wait_send())
-        swap.wait_send()
 
     for layer in range(layers):
         layer_step(layer, tok_ref if layer == 0 else hid.at[layer - 1], hid.at[layer])
-    out_ref[...] = hid[layers - 1]
+    for copy in gain_copies:
+        copy.wait_send()
 
     pl.when(me < n - 1)(doc_copy.wait_send)
 
@@ -350,15 +382,14 @@
 
                 @pl.loop(1 if way else 0, half_n + 1 if piece == way else half_n)
                 def _(step, layer=layer, way=way, piece=piece):
-                    for pair in range(pairs):
-                        part = owner_at(way, step) // half_n
+                    for k in range(1, pairs):
                         ref = held(layer, 2, me, piece)
-                        copy = to_tp(ref, ref, osend.at[layer, way, step, piece, pair],
-                                     orecv.at[layer, t, 0], 2 * ((q + pair) % pairs) + part)
-                        if pair == 0:
-                            pl.when(part != c)(copy.wait_send)
-                        else:
-                            copy.wait_send()
+                        to_tp(ref, ref, osend.at[layer, way, step, piece, k - 1],
+                              orecv.at[layer, q, 0], 2 * ((q + k) % pairs) + c).wait_send()
+
+    for chunk in range(chunks):
+        span = pl.ds(chunk * 128, 128)
+        pltpu.make_async_copy(hid.at[layers - 1, span], out_ref.at[span], wsem.at[chunk]).wait()
 
 
 def fused_on_device(n, m, tokens, doc_ids, pre_gain, value_proj, gate_proj, out_proj, conv_taps, norm_gain, norm_shift):
@@ -366,7 +397,7 @@
     layers, depth, block = value_proj.shape
     owidth = out_proj.shape[2]
     reach = conv_taps.shape[1] - 1
-    channels = block * m
+    pairs, chunks = m // 2, rows // 128
     docs = doc_ids.reshape(rows // 128, 128)
     bf16, f32, i32 = jnp.bfloat16, jnp.float32, jnp.int32
     dma = pltpu.SemaphoreType.DMA
@@ -375,11 +406,10 @@
         functools.partial(fused_kernel, n, m, reach, layers),
         out_shape=jax.ShapeDtypeStruct((rows, width), bf16),
         in_specs=[vmem] * 9,
-        out_specs=vmem,
+        out_specs=pl.BlockSpec(memory_space=pl.ANY),
         scratch_shapes=[
             pltpu.VMEM((layers, 2, n * depth, block), bf16),
-            pltpu.VMEM((layers, block, n * owidth), bf16),
-            pltpu.VMEM((layers, channels, width // 2), bf16),
+            pltpu.VMEM((layers, pairs * block, n * owidth), bf16),
             pltpu.VMEM((rows, width), bf16),
             pltpu.VMEM((rows, block), f32),
             pltpu.VMEM((2, rows + HALO, block // 2), f32),
@@ -390,17 +420,21 @@
             pltpu.VMEM((HALO, 128), f32),
             pltpu.VMEM((HALO, 128), f32),
             pltpu.VMEM((rows, 128), f32),
-            pltpu.VMEM((layers, 8, rows), f32),
-            pltpu.VMEM((layers, m, 8, rows), f32),
-            pltpu.VMEM((rows, block), f32),
-            pltpu.VMEM((layers, rows, channels), bf16),
+            pltpu.VMEM((layers, m, chunks, 8, 128), f32),
+            pltpu.VMEM((pairs, layers, block), f32),
+            pltpu.VMEM((pairs, layers, block), f32),
+            pltpu.VMEM((layers, pairs, rows, block), bf16),
+            pltpu.VMEM((rows, pairs * block), bf16),
+            pltpu.VMEM((layers, rows, width), bf16),
+            pltpu.VMEM((layers, rows, width), bf16),
             pltpu.VMEM((layers, rows, width), bf16),
             dma((layers, 3, 2, n // 2, 2)), dma((layers, 3, 2, n // 2, 2)),
-            dma((layers, 2, n // 2 + 1, 2, m // 2)), dma((layers, m, n)),
+            dma((layers, 2, n // 2 + 1, 2, pairs)), dma((layers, pairs, 2 * n)),
             dma((2 * layers + 1,)), dma((2 * layers + 1,)),
-            dma((layers, m)), dma((layers, m)),
-            dma((layers, m)), dma((layers, m)),
-            dma((layers,)), dma((layers,)),
+            dma((layers, m, chunks)), dma((layers, m, chunks)),
+            dma((layers, pairs, chunks + 1)), dma((layers, pairs, chunks + 1)),
+            dma((layers, chunks)), dma((layers, chunks)),
+            dma((pairs, 2)), dma((pairs, 2)), dma((chunks,)),
         ],
         compiler_params=pltpu.CompilerParams(
             collective_id=0, has_side_effects=True, vmem_limit_bytes=60 * 1024 * 1024),

time: 104 us -> 94 us (0.904); the launches traced: 104 us -> 93 us
  Pallas kernels: 101 us -> 90.2 us
    pallas_call x1, Pallas kernels: 101 us -> 90.2 us  [fused_on_device(): pl.pallas_call(functools.partial(fused_kernel, n, m, reach, layers), out_...]
where the time goes in v2:
time: 94 us; the launch traced here: 93 us
  Pallas kernels  90.2 us (96%)
  local copies, waits for them, and re-layouts  2.73 us (3%)
    pallas_call x1, Pallas kernels, fused_on_device(): pl.pallas_call(functools.partial(fused_kernel, n, m, reach, layers), out_...  90.2 us
    unnamed x1, local copies, waits for them, and re-layouts  2.73 us

profile of v2, /device:TPU:9, one launch (start us, length us, event | category | flops | bytes accessed | tf_op | source)
XLA Modules:
  0.0 93.0 jit_solution(17645805799084487898)
XLA Ops:
  0.0 90.2 %shard_map.91 = bf16[384,2048]{1,0:T(8,128)(2,1)} custom-call(bf16[384,2048]{1,0:T(8,128)(2,1)} %tok_ref.1, s32[3,128]{1,0:T(4,128)} %bitcast.3, f32[2,2048]{1,0:T(2,128)} %gain_ref.1, bf16[2,256,256]{2,1,0:T(8,128)(2,1)} %v_ref.1, bf16[2,256,256]{2,1,0:T(8,128)(2,1)} %g_ref.1, bf16[2,256,256]{2,1,0:T(8,128)(2,1)} %o_ref.1, f32[31,2,256]{2,1,0:T(2,128)} %bitcast.2, ...), custom_call_target="tpu_custom_call" | custom-call | tf_op jit(solution)/shard_map/pallas_call | solution.py:405
  90.3 2.7 %copy.11 = bf16[384,2048]{1,0:T(8,128)(2,1)} copy(bf16[384,2048]{1,0:T(8,128)(2,1)} %shard_map.91) | data formatting | bytes 3145728

commit v3 on v2

--- a/solution.py
+++ b/solution.py
@@ -14,11 +14,11 @@
 
 def fused_kernel(
     n, m, reach, layers,
-    tok_ref, doc_ref, gain_ref, v_ref, g_ref, o_ref, tap_ref, ng_ref, ns_ref,
-    out_ref,
+    tok_hbm, doc_hbm, gain_hbm, v_hbm, g_hbm, o_hbm, tap_hbm, ng_hbm, ns_hbm,
+    out_ref, tok_ref, doc_ref, gain_ref, v_ref, g_ref, o_ref, tap_ref, ng_ref, ns_ref,
     w, oall, normed, acc, padded, pdoc, run, ghalo, halo_in, doc_in, doc_tail,
     stat, stats, ng_all, ns_all, conv, act, psend, precv, hid,
-    rsend, rrecv, osend, orecv, hsend, hrecv, ssend, srecv, csend, crecv, xsend, xrecv, gsend, grecv, wsem,
+    rsend, rrecv, osend, orecv, hsend, hrecv, ssend, srecv, csend, crecv, xsend, xrecv, gsend, grecv, lsem,
 ):
     me = lax.axis_index("sp")
     t = lax.axis_index("tp")
@@ -44,6 +44,11 @@
         pl.semaphore_signal(barrier, inc=1, device_id={"sp": other}, device_id_type=MESH)
     for k in range(1, m):
         pl.semaphore_signal(barrier, inc=1, device_id={"tp": (t + k) % m}, device_id_type=MESH)
+    loads = [pltpu.make_async_copy(src, dst, lsem.at[index]) for index, (src, dst) in enumerate(
+        ((v_hbm, v_ref), (g_hbm, g_ref), (o_hbm, o_ref), (ng_hbm, ng_ref), (ns_hbm, ns_ref),
+         (tok_hbm, tok_ref), (gain_hbm, gain_ref), (doc_hbm, doc_ref), (tap_hbm, tap_ref)))]
+    for load in loads:
+        load.start()
     pl.semaphore_wait(barrier, 1 + m)
 
     def to_sp(src, dst, send, recv, target):
@@ -71,20 +76,18 @@
         return o_ref.at[layer, :, pl.ds(piece * ho, ho)]
 
     def ring_copy(layer, kind, way, step, piece, src, dst):
-        return to_sp(src, dst, rsend.at[layer, kind, way, step, piece], rrecv.at[layer, kind, way, step, piece],
+        return to_sp(src, dst, rsend.at[layer, kind], rrecv.at[layer, kind, way, step, piece],
                      right if way == 0 else left)
 
     def travels(way, step, piece):
         return step < half_n - 1 or piece == way
 
-    def spread(layer, way, step, piece, act):
+    def spread(layer, way, step, piece):
         owner = owner_at(way, step)
         part = held(layer, 2, owner, piece)
         src = own_piece(layer, 2, piece) if step == 0 else part
         for k in range(1, pairs):
-            copy = to_tp(src, part, osend.at[layer, way, step, piece, k - 1],
-                         orecv.at[layer, q, owner * 2 + piece], 2 * ((q + k) % pairs) + c)
-            getattr(copy, act)()
+            to_tp(src, part, osend.at[layer, k], orecv.at[layer, q], 2 * ((q + k) % pairs) + c).start()
 
     def advance_one(layer, kind, step):
         for turn in range(2):
@@ -98,15 +101,17 @@
                     dst = held(layer, kind, owner_at(way, step), piece)
                     src = own_piece(layer, kind, piece) if step == 0 else dst
                     ring_copy(layer, kind, way, step, piece, src, dst).start()
-                if kind == 2 and arrived and (step > 0 or way == 0):
-                    spread(layer, way, step, piece, "start")
+                if kind == 2 and arrived and step > 0:
+                    spread(layer, way, step, piece)
 
     entries = []
     for layer in range(layers):
         for step in range(half_n + 1):
-            entries.append((11 * layer + 3.3 * step, layer, 0, step))
-            entries.append((11 * layer + (2 if layer else 1) + 3.3 * step, layer, 1, step))
-            entries.append((11 * layer + (2.5 if layer else 5) + 3.2 * step, layer, 2, step))
+            for kind, (first, base, pace) in enumerate(
+                    ((10.5, 10.5, 3.5), (13.5, 11.9, 3.4), (12.2, 11.5, 3.4)) if layer
+                    else ((0, 0, 3), (1, 1, 3), (0.5, 0.5, 3))):
+                shift = 11.5 * max(layer - 1, 0)
+                entries.append((shift + (base + pace * step if step else first), layer, kind, step))
     pending = [entry[1:] for entry in sorted(entries)]
 
     def tend(count):
@@ -117,6 +122,17 @@
     def advance(*target):
         while target in pending:
             advance_one(*pending.pop(0))
+
+    def drain(layer):
+        for kind in range(3):
+            if kind < 2:
+                ref = w.at[layer, kind, pl.ds(0, (n - 1) * depth)]
+            else:
+                ref = oall.at[layer, pl.ds(pl.multiple_of(q * block, block), block), pl.ds(0, (n - 1) * owidth)]
+            to_sp(ref, ref, rsend.at[layer, kind], rrecv.at[layer, kind, 0, 0, 0], right).wait_send()
+        for k in range(1, pairs):
+            ref = oall.at[layer, pl.ds(pl.multiple_of(q * block, block), block)]
+            to_tp(ref, ref, osend.at[layer, k], orecv.at[layer, q], 2 * ((q + k) % pairs) + c).wait_send()
 
     def keep_own(layer):
         row = pl.ds(pl.multiple_of(me * depth, depth), depth)
@@ -126,7 +142,12 @@
         oall[layer, pl.ds(pl.multiple_of(q * block, block), block),
              pl.ds(pl.multiple_of(me * owidth, owidth), owidth)] = o_ref[layer]
 
-    tend(2)
+    for load in loads[:5]:
+        load.wait()
+    tend(3)
+    for layer in range(layers):
+        for piece in range(2):
+            spread(layer, 0, 0, piece)
     gain_copies = []
     for k in range(1, pairs):
         for index, (src, dst) in enumerate(((ng_ref, ng_all), (ns_ref, ns_all))):
@@ -135,6 +156,9 @@
             gain_copies.append(copy)
     ng_all[q] = ng_ref[...]
     ns_all[q] = ns_ref[...]
+
+    for load in loads[5:]:
+        load.wait()
 
     def doc_block(i):
         row = doc_ref[pl.ds(i, 1), :].astype(jnp.float32)
@@ -275,21 +299,21 @@
         if layer == 0:
             pl.when(me < n - 1)(doc_copy.start)
         gate_half(0)
+        pause()
         if last:
-            tend(1)
+            advance(layer, 2, half_n)
             first_half()
+        if layer == 0:
+            advance(layer, 2, half_n)
+            count_runs()
         advance(layer, 1, half_n)
         gate_half(1)
-        if last:
-            advance(layer, 2, half_n)
-        else:
-            if layer == 0:
-                count_runs()
+        pause()
+        if not last:
+            first_half()
             pause()
-            first_half()
         for chunk in order:
             if chunk == 0:
-                pause()
                 take_halo(1)
             conv_rows(1, 2 * chunk, 2 * chunk + 2)
             stats[layer, t, chunk] = jnp.transpose(stat[pl.ds(chunk * 128, 128), :])[:8]
@@ -297,7 +321,6 @@
                 stat_copy(chunk, k, t).start()
             conv_copies(1, chunk, q, "start")
 
-        pause()
         pause()
         gains = [ng_all[p, pl.ds(layer, 1), :] for p in range(pairs)]
         shifts = [ns_all[p, pl.ds(layer, 1), :] for p in range(pairs)]
@@ -319,22 +342,23 @@
                 normalized = gains[p] * (conv[layer, p, span, :].astype(jnp.float32) - row_mean) * row_scale + shifts[p]
                 act[span, pl.ds(p * block, block)] = jax.nn.silu(normalized).astype(jnp.bfloat16)
             if chunk == order[0]:
-                if not last:
-                    pause()
-                    advance(layer, 2, half_n)
                 for k in range(1, pairs):
                     peer = (q + k) % pairs
-
-                    @pl.loop(0, 2 * n)
-                    def _(piece, peer=peer):
-                        part = oall.at[layer, pl.ds(pl.multiple_of(peer * block, block), block),
-                                       pl.ds(pl.multiple_of(piece * ho, ho), ho)]
-                        to_tp(part, part, osend.at[layer, 0, 0, 0, 0], orecv.at[layer, peer, piece], t).wait_recv()
+                    part = oall.at[layer, pl.ds(pl.multiple_of(peer * block, block), block)]
+                    to_tp(part, part, osend.at[layer, k], orecv.at[layer, peer], t).wait_recv()
             psend[layer, span, :] = jnp.dot(
                 act[span, :], oall[layer], preferred_element_type=jnp.float32).astype(jnp.bfloat16)
             swap_copy(chunk).start()
-            pause()
-
+            if chunk == order[0]:
+                pause()
+
+        pause()
+        if last:
+            for each in range(layers):
+                drain(each)
+            for copy in gain_copies:
+                copy.wait_send()
+            pl.when(me < n - 1)(doc_copy.wait_send)
         for chunk in order:
             swap_copy(chunk).wait_recv()
 
@@ -350,11 +374,6 @@
                     scale = lax.rsqrt(jnp.mean(wide * wide, axis=-1, keepdims=True) + epsilon)
                     normed[span, :] = (wide * scale * gain_ref[pl.ds(layer + 1, 1), :]).astype(jnp.bfloat16)
 
-            if last:
-                span = pl.ds(chunk * 128, 128)
-                pltpu.make_async_copy(target.at[span], out_ref.at[span], wsem.at[chunk]).start()
-            pause()
-
         for chunk in range(chunks):
             for k in range(1, m):
                 stat_copy(chunk, k, t).wait_send()
@@ -365,31 +384,8 @@
             pl.when(me < n - 1)(lambda kind=kind: halo_copy(kind).wait_send())
 
     for layer in range(layers):
-        layer_step(layer, tok_ref if layer == 0 else hid.at[layer - 1], hid.at[layer])
-    for copy in gain_copies:
-        copy.wait_send()
-
-    pl.when(me < n - 1)(doc_copy.wait_send)
-
-    for layer in range(layers):
-        for way in range(2):
-            for piece in range(2):
-                for kind in range(3):
-                    @pl.loop(0, half_n if piece == way else half_n - 1)
-                    def _(step, layer=layer, way=way, piece=piece, kind=kind):
-                        ref = held(layer, kind, me, piece)
-                        ring_copy(layer, kind, way, step, piece, ref, ref).wait_send()
-
-                @pl.loop(1 if way else 0, half_n + 1 if piece == way else half_n)
-                def _(step, layer=layer, way=way, piece=piece):
-                    for k in range(1, pairs):
-                        ref = held(layer, 2, me, piece)
-                        to_tp(ref, ref, osend.at[layer, way, step, piece, k - 1],
-                              orecv.at[layer, q, 0], 2 * ((q + k) % pairs) + c).wait_send()
-
-    for chunk in range(chunks):
-        span = pl.ds(chunk * 128, 128)
-        pltpu.make_async_copy(hid.at[layers - 1, span], out_ref.at[span], wsem.at[chunk]).wait()
+        layer_step(layer, tok_ref if layer == 0 else hid.at[layer - 1],
+                   out_ref if layer + 1 == layers else hid.at[layer])
 
 
 def fused_on_device(n, m, tokens, doc_ids, pre_gain, value_proj, gate_proj, out_proj, conv_taps, norm_gain, norm_shift):
@@ -402,12 +398,16 @@
     bf16, f32, i32 = jnp.bfloat16, jnp.float32, jnp.int32
     dma = pltpu.SemaphoreType.DMA
     vmem = pl.BlockSpec(memory_space=pltpu.VMEM)
+    hbm = pl.BlockSpec(memory_space=pltpu.HBM)
     return pl.pallas_call(
         functools.partial(fused_kernel, n, m, reach, layers),
-        out_shape=jax.ShapeDtypeStruct((rows, width), bf16),
-        in_specs=[vmem] * 9,
-        out_specs=pl.BlockSpec(memory_space=pl.ANY),
+        out_shape=pltpu.VMEM((rows, width), bf16),
+        in_specs=[hbm] * 9,
+        out_specs=vmem,
         scratch_shapes=[
+            pltpu.VMEM((rows, width), bf16), pltpu.VMEM(docs.shape, i32), pltpu.VMEM(pre_gain.shape, f32),
+            pltpu.VMEM(value_proj.shape, bf16), pltpu.VMEM(gate_proj.shape, bf16), pltpu.VMEM(out_proj.shape, bf16),
+            pltpu.VMEM((reach + 1, layers, block), f32), pltpu.VMEM(norm_gain.shape, f32), pltpu.VMEM(norm_shift.shape, f32),
             pltpu.VMEM((layers, 2, n * depth, block), bf16),
             pltpu.VMEM((layers, pairs * block, n * owidth), bf16),
             pltpu.VMEM((rows, width), bf16),
@@ -427,14 +427,14 @@
             pltpu.VMEM((rows, pairs * block), bf16),
             pltpu.VMEM((layers, rows, width), bf16),
             pltpu.VMEM((layers, rows, width), bf16),
-            pltpu.VMEM((layers, rows, width), bf16),
-            dma((layers, 3, 2, n // 2, 2)), dma((layers, 3, 2, n // 2, 2)),
-            dma((layers, 2, n // 2 + 1, 2, pairs)), dma((layers, pairs, 2 * n)),
+            pltpu.VMEM((max(1, layers - 1), rows, width), bf16),
+            dma((layers, 3)), dma((layers, 3, 2, n // 2, 2)),
+            dma((layers, pairs)), dma((layers, pairs)),
             dma((2 * layers + 1,)), dma((2 * layers + 1,)),
             dma((layers, m, chunks)), dma((layers, m, chunks)),
             dma((layers, pairs, chunks + 1)), dma((layers, pairs, chunks + 1)),
             dma((layers, chunks)), dma((layers, chunks)),
-            dma((pairs, 2)), dma((pairs, 2)), dma((chunks,)),
+            dma((pairs, 2)), dma((pairs, 2)), dma((9,)),
         ],
         compiler_params=pltpu.CompilerParams(
             collective_id=0, has_side_effects=True, vmem_limit_bytes=60 * 1024 * 1024),

time: 94 us -> 79.2 us (0.84)
  Pallas kernels: 90.2 us -> 77.8 us
  local copies, waits for them, and re-layouts: 2.73 us -> 1.15 us
    pallas_call x1, Pallas kernels: 90.2 us -> 77.8 us  [fused_on_device(): pl.pallas_call(functools.partial(fused_kernel, n, m, reach, layers), out_...]
    unnamed x1, local copies, waits for them, and re-layouts: 2.73 us -> 1.15 us
where the time goes in v3:
time: 79.2 us; the launch traced here: 79 us
  Pallas kernels  77.8 us (98%)
  local copies, waits for them, and re-layouts  1.15 us (1%)
    pallas_call x1, Pallas kernels, fused_on_device(): pl.pallas_call(functools.partial(fused_kernel, n, m, reach, layers), out_...  77.8 us

profile of v3, /device:TPU:9, one launch (start us, length us, event | category | flops | bytes accessed | tf_op | source)
XLA Modules:
  0.0 79.0 jit_solution(6843278788564113032)
XLA Ops:
  0.0 77.8 %shard_map.91 = bf16[384,2048]{1,0:T(8,128)(2,1)S(1)} custom-call(bf16[384,2048]{1,0:T(8,128)(2,1)} %tok_hbm.1, s32[3,128]{1,0:T(4,128)} %bitcast.3, f32[2,2048]{1,0:T(2,128)} %gain_hbm.1, bf16[2,256,256]{2,1,0:T(8,128)(2,1)} %v_hbm.1, bf16[2,256,256]{2,1,0:T(8,128)(2,1)} %g_hbm.1, bf16[2,256,256]{2,1,0:T(8,128)(2,1)} %o_hbm.1, f32[31,2,256]{2,1,0:T(2,128)} %bitcast.2, ...), custom_call_target="tpu_custom_call" | custom-call | tf_op jit(solution)/shard_map/pallas_call | solution.py:402
  77.8 1.1 %copy.11 = bf16[384,2048]{1,0:T(8,128)(2,1)} copy(bf16[384,2048]{1,0:T(8,128)(2,1)S(1)} %shard_map.91) | data formatting | bytes 3145728

commit v4 on v3

--- a/solution.py
+++ b/solution.py
@@ -10,6 +10,8 @@
 MESH = pl.DeviceIdType.MESH
 HALO = 32
 CONV_ROWS = 64
+GATE_ROWS = 64
+MARKS = [2, 1, 1, 1, 1, 1, 1]
 
 
 def fused_kernel(
@@ -17,7 +19,7 @@
     tok_hbm, doc_hbm, gain_hbm, v_hbm, g_hbm, o_hbm, tap_hbm, ng_hbm, ns_hbm,
     out_ref, tok_ref, doc_ref, gain_ref, v_ref, g_ref, o_ref, tap_ref, ng_ref, ns_ref,
     w, oall, normed, acc, padded, pdoc, run, ghalo, halo_in, doc_in, doc_tail,
-    stat, stats, ng_all, ns_all, conv, act, psend, precv, hid,
+    stat, stats, scales, conv, act, psend, precv, hid,
     rsend, rrecv, osend, orecv, hsend, hrecv, ssend, srecv, csend, crecv, xsend, xrecv, gsend, grecv, lsem,
 ):
     me = lax.axis_index("sp")
@@ -64,51 +66,52 @@
     def owner_at(way, distance):
         return index_of(my_pos - distance if way == 0 else my_pos + distance)
 
-    def held(layer, kind, owner, piece):
+    def held(layer, kind, owner, first=0, count=2):
         if kind < 2:
-            return w.at[layer, kind, pl.ds(pl.multiple_of(owner * depth, depth), depth), pl.ds(piece * hb, hb)]
+            return w.at[layer, kind, pl.ds(pl.multiple_of(owner * depth, depth), depth), pl.ds(first * hb, count * hb)]
         return oall.at[layer, pl.ds(pl.multiple_of(q * block, block), block),
-                       pl.ds(pl.multiple_of(owner * owidth + piece * ho, ho), ho)]
-
-    def own_piece(layer, kind, piece):
+                       pl.ds(pl.multiple_of(owner * owidth + first * ho, ho), count * ho)]
+
+    def several(layer, kind, count):
         if kind < 2:
-            return (v_ref, g_ref)[piece].at[layer, :, pl.ds(kind * hb, hb)]
-        return o_ref.at[layer, :, pl.ds(piece * ho, ho)]
-
-    def ring_copy(layer, kind, way, step, piece, src, dst):
-        return to_sp(src, dst, rsend.at[layer, kind], rrecv.at[layer, kind, way, step, piece],
-                     right if way == 0 else left)
-
-    def travels(way, step, piece):
-        return step < half_n - 1 or piece == way
-
-    def spread(layer, way, step, piece):
-        owner = owner_at(way, step)
-        part = held(layer, 2, owner, piece)
-        src = own_piece(layer, 2, piece) if step == 0 else part
-        for k in range(1, pairs):
-            to_tp(src, part, osend.at[layer, k], orecv.at[layer, q], 2 * ((q + k) % pairs) + c).start()
+            return w.at[layer, kind, pl.ds(0, count * depth)]
+        return oall.at[layer, pl.ds(pl.multiple_of(q * block, block), block), pl.ds(0, count * owidth)]
+
+    def ring_copy(layer, kind, way, step, src, dst):
+        return to_sp(src, dst, rsend.at[layer, kind], rrecv.at[layer, kind, step], right if way == 0 else left)
+
+    def spread_copy(layer, k, src, dst):
+        return to_tp(src, dst, osend.at[layer, k], orecv.at[layer, q], 2 * ((q + k) % pairs) + c)
 
     def advance_one(layer, kind, step):
-        for turn in range(2):
-            for way in range(2):
-                piece = turn ^ way
-                arrived = step == 0 or travels(way, step - 1, piece)
-                if step > 0 and arrived:
-                    piece_ref = held(layer, kind, owner_at(way, step), piece)
-                    ring_copy(layer, kind, way, step - 1, piece, piece_ref, piece_ref).wait_recv()
-                if step < half_n and travels(way, step, piece):
-                    dst = held(layer, kind, owner_at(way, step), piece)
-                    src = own_piece(layer, kind, piece) if step == 0 else dst
-                    ring_copy(layer, kind, way, step, piece, src, dst).start()
-                if kind == 2 and arrived and step > 0:
-                    spread(layer, way, step, piece)
+        if step > 0:
+            landed = several(layer, kind, 2 if step < half_n else 1)
+            ring_copy(layer, kind, 0, step - 1, landed, landed).wait_recv()
+        for way in range(2):
+            owner = owner_at(way, step)
+            first, count = (0, 2) if step < half_n - 1 else (way, 1)
+            if step == half_n:
+                continue
+            dst = held(layer, kind, owner, first, count)
+            if step > 0:
+                ring_copy(layer, kind, way, step, dst, dst).start()
+            elif kind == 2:
+                ring_copy(layer, kind, way, step, o_ref.at[layer, :, pl.ds(first * ho, count * ho)], dst).start()
+            else:
+                for piece in range(first, first + count):
+                    ring_copy(layer, kind, way, step, (v_ref, g_ref)[piece].at[layer, :, pl.ds(kind * hb, hb)],
+                              held(layer, kind, owner, piece, 1)).start()
+        if kind == 2 and step > 0:
+            for way in range(2 if step < half_n else 1):
+                for k in range(1, pairs):
+                    part = held(layer, 2, owner_at(way, step))
+                    spread_copy(layer, k, part, part).start()
 
     entries = []
     for layer in range(layers):
         for step in range(half_n + 1):
             for kind, (first, base, pace) in enumerate(
-                    ((10.5, 10.5, 3.5), (13.5, 11.9, 3.4), (12.2, 11.5, 3.4)) if layer
+                    ((12.2, 11.7, 3.2), (12.3, 12.7, 3.2), (10.5, 11.2, 2.9)) if layer
                     else ((0, 0, 3), (1, 1, 3), (0.5, 0.5, 3))):
                 shift = 11.5 * max(layer - 1, 0)
                 entries.append((shift + (base + pace * step if step else first), layer, kind, step))
@@ -125,14 +128,11 @@
 
     def drain(layer):
         for kind in range(3):
-            if kind < 2:
-                ref = w.at[layer, kind, pl.ds(0, (n - 1) * depth)]
-            else:
-                ref = oall.at[layer, pl.ds(pl.multiple_of(q * block, block), block), pl.ds(0, (n - 1) * owidth)]
-            to_sp(ref, ref, rsend.at[layer, kind], rrecv.at[layer, kind, 0, 0, 0], right).wait_send()
+            ref = several(layer, kind, n - 1)
+            ring_copy(layer, kind, 0, 0, ref, ref).wait_send()
         for k in range(1, pairs):
-            ref = oall.at[layer, pl.ds(pl.multiple_of(q * block, block), block)]
-            to_tp(ref, ref, osend.at[layer, k], orecv.at[layer, q], 2 * ((q + k) % pairs) + c).wait_send()
+            ref = several(layer, 2, n)
+            spread_copy(layer, k, ref, ref).wait_send()
 
     def keep_own(layer):
         row = pl.ds(pl.multiple_of(me * depth, depth), depth)
@@ -146,16 +146,15 @@
         load.wait()
     tend(3)
     for layer in range(layers):
-        for piece in range(2):
-            spread(layer, 0, 0, piece)
+        for k in range(1, pairs):
+            spread_copy(layer, k, o_ref.at[layer], held(layer, 2, me)).start()
     gain_copies = []
     for k in range(1, pairs):
-        for index, (src, dst) in enumerate(((ng_ref, ng_all), (ns_ref, ns_all))):
-            copy = to_tp(src, dst.at[q], gsend.at[k, index], grecv.at[q, index], 2 * ((q + k) % pairs) + c)
-            copy.start()
-            gain_copies.append(copy)
-    ng_all[q] = ng_ref[...]
-    ns_all[q] = ns_ref[...]
+        for index, src in enumerate((ng_ref, ns_ref)):
+            to_tp(src, scales.at[q, index], gsend.at[k], grecv.at[q], 2 * ((q + k) % pairs) + c).start()
+        gain_copies.append(to_tp(scales.at[q], scales.at[q], gsend.at[k], grecv.at[q], 2 * ((q + k) % pairs) + c))
+    scales[q, 0] = ng_ref[...]
+    scales[q, 1] = ns_ref[...]
 
     for load in loads[5:]:
         load.wait()
@@ -190,9 +189,8 @@
 
     def count_runs():
         for k in range(1, pairs):
-            for index, dst in enumerate((ng_all, ns_all)):
-                peer = (q + k) % pairs
-                to_tp(dst.at[peer], dst.at[peer], gsend.at[k, index], grecv.at[peer, index], t).wait_recv()
+            peer = (q + k) % pairs
+            to_tp(scales.at[peer], scales.at[peer], gsend.at[k], grecv.at[peer], 2 * peer + c).wait_recv()
 
         @pl.when(me > 0)
         def _():
@@ -215,7 +213,7 @@
 
     def layer_step(layer, source, target):
         last = layer + 1 == layers
-        marks = [1, 1, 1, 1, 1, 1, 1, 1, 1]
+        marks = MARKS[:]
 
         def pause():
             if not last and marks:
@@ -225,37 +223,32 @@
             return to_sp(ghalo.at[layer, kind], halo_in.at[layer, kind],
                          hsend.at[2 * layer + kind], hrecv.at[2 * layer + kind], following)
 
-        def store_padded(kind, row, values):
-            padded[kind, pl.ds(row, 32), :] = values.astype(jnp.float32)
-
         def gate_half(kind):
             acc[...] = jnp.dot(normed[...], w[layer, kind], preferred_element_type=jnp.float32)
 
-            def gate_rows(i):
-                span = pl.ds(pl.multiple_of(i * 32, 32), 32)
+            def gate_rows(start):
+                span = pl.ds(start, GATE_ROWS)
                 value = acc[span, pl.ds(0, hb)].astype(jnp.bfloat16).astype(jnp.float32)
                 gate = acc[span, pl.ds(hb, hb)].astype(jnp.bfloat16).astype(jnp.float32)
                 gated = (value * jax.nn.sigmoid(gate)).astype(jnp.bfloat16)
-                store_padded(kind, pl.multiple_of(i * 32 + HALO, 32), gated)
+                padded[kind, pl.ds(start + HALO, GATE_ROWS), :] = gated.astype(jnp.float32)
                 return gated
 
-            ghalo[layer, kind] = gate_rows(rows // 32 - 1)
+            ghalo[layer, kind] = gate_rows(rows - GATE_ROWS)[GATE_ROWS - HALO:]
             pl.when(me < n - 1)(lambda: halo_copy(kind).start())
 
-            @pl.loop(0, rows // 32 - 1)
-            def _(i):
-                gate_rows(i)
+            for i in range(rows // GATE_ROWS - 1):
+                gate_rows(i * GATE_ROWS)
 
         def take_halo(kind):
             pl.when(me > 0)(lambda: halo_copy(kind).wait_recv())
-            store_padded(kind, 0, halo_in[layer, kind])
+            padded[kind, pl.ds(0, HALO), :] = halo_in[layer, kind].astype(jnp.float32)
 
         def conv_rows(kind, first, end):
             cols = pl.ds(kind * hb, hb)
 
-            @pl.loop(first, end)
-            def _(i):
-                base = pl.multiple_of(i * CONV_ROWS, CONV_ROWS)
+            for i in range(first, end):
+                base = i * CONV_ROWS
                 span = pl.ds(base, CONV_ROWS)
                 count = run[span, :]
                 total = tap_ref[0, pl.ds(layer, 1), cols] * padded[kind, pl.ds(base + HALO, CONV_ROWS), :]
@@ -270,78 +263,80 @@
                     sums = sums + stat[span, :]
                 stat[span, :] = sums
 
-        def conv_copies(kind, chunk, p, act):
-            span = pl.ds(chunk * 128, 128) if kind else pl.ds(0, rows)
-            slot = chunk + 1 if kind else 0
+        def conv_copies(kind, chunk):
+            part = conv.at[layer, q, pl.ds(chunk * 128, 128), pl.ds(kind * hb, hb)]
             for k in range(1, pairs):
-                peer = (q + k) % pairs
-                part = conv.at[layer, p if p is not None else peer, span, pl.ds(kind * hb, hb)]
-                copy = to_tp(part, part, csend.at[layer, k, slot],
-                             crecv.at[layer, p if p is not None else peer, slot], 2 * peer + c)
-                getattr(copy, act)()
-
-        def stat_copy(chunk, k, who):
-            part = stats.at[layer, who, chunk]
-            return to_tp(part, part, ssend.at[layer, k, chunk], srecv.at[layer, who, chunk], (t + k) % m)
+                to_tp(part, part, csend.at[layer], crecv.at[layer, chunk], 2 * ((q + k) % pairs) + c).start()
+
+        def conv_landed(chunk):
+            part = conv.at[layer, pl.ds(0, pairs - 1), pl.ds(chunk * 128, 128)]
+            return to_tp(part, part, csend.at[layer], crecv.at[layer, chunk], partner)
+
+        def stat_copies(chunk):
+            part = stats.at[layer, chunk, t]
+            for k in range(1, m):
+                to_tp(part, part, ssend.at[layer], srecv.at[layer, chunk], (t + k) % m).start()
+
+        def stats_landed(chunk):
+            part = stats.at[layer, chunk, pl.ds(0, m - 1)]
+            return to_tp(part, part, ssend.at[layer], srecv.at[layer, chunk], partner)
 
         def swap_copy(chunk):
             span = pl.ds(chunk * 128, 128)
-            return to_tp(psend.at[layer, span], precv.at[layer, span], xsend.at[layer, chunk],
+            return to_tp(psend.at[layer, span], precv.at[layer, span], xsend.at[layer],
                          xrecv.at[layer, chunk], partner)
 
-        def first_half():
-            conv_rows(0, 1, rows // CONV_ROWS)
-            take_halo(0)
-            conv_rows(0, 0, 1)
-            conv_copies(0, 0, q, "start")
+        def first_rows(chunk):
+            conv_rows(0, 2 * chunk, 2 * chunk + 2)
+            conv_copies(0, chunk)
 
         advance(layer, 0, half_n)
         if layer == 0:
             pl.when(me < n - 1)(doc_copy.start)
         gate_half(0)
-        pause()
-        if last:
-            advance(layer, 2, half_n)
-            first_half()
         if layer == 0:
             advance(layer, 2, half_n)
+            pause()
             count_runs()
+        if last:
+            for chunk in order[:-1]:
+                first_rows(chunk)
         advance(layer, 1, half_n)
         gate_half(1)
-        pause()
         if not last:
-            first_half()
             pause()
+            for chunk in order[:-1]:
+                first_rows(chunk)
         for chunk in order:
             if chunk == 0:
+                take_halo(0)
+                first_rows(0)
+                pause()
                 take_halo(1)
             conv_rows(1, 2 * chunk, 2 * chunk + 2)
-            stats[layer, t, chunk] = jnp.transpose(stat[pl.ds(chunk * 128, 128), :])[:8]
-            for k in range(1, m):
-                stat_copy(chunk, k, t).start()
-            conv_copies(1, chunk, q, "start")
+            stats[layer, chunk, t] = jnp.transpose(stat[pl.ds(chunk * 128, 128), :])[:8]
+            stat_copies(chunk)
+            conv_copies(1, chunk)
 
         pause()
-        gains = [ng_all[p, pl.ds(layer, 1), :] for p in range(pairs)]
-        shifts = [ns_all[p, pl.ds(layer, 1), :] for p in range(pairs)]
+        gains = [scales[p, 0, pl.ds(layer, 1), :] for p in range(pairs)]
+        shifts = [scales[p, 1, pl.ds(layer, 1), :] for p in range(pairs)]
         for chunk in order:
-            for k in range(1, m):
-                stat_copy(chunk, k, (t + k) % m).wait_recv()
-            summed = stats[layer, 0, chunk]
+            stats_landed(chunk).wait_recv()
+            summed = stats[layer, chunk, 0]
             for who in range(1, m):
-                summed = summed + stats[layer, who, chunk]
+                summed = summed + stats[layer, chunk, who]
             both = jnp.transpose(jnp.concatenate([summed, jnp.zeros((120, 128), jnp.float32)], axis=0))
             row_mean = both[:, 0:1] / channels
             row_var = both[:, 1:2] / channels - row_mean * row_mean
             row_scale = lax.rsqrt(row_var + epsilon)
-            if chunk == order[0]:
-                conv_copies(0, 0, None, "wait_recv")
-            conv_copies(1, chunk, None, "wait_recv")
+            conv_landed(chunk).wait_recv()
             span = pl.ds(chunk * 128, 128)
             for p in range(pairs):
                 normalized = gains[p] * (conv[layer, p, span, :].astype(jnp.float32) - row_mean) * row_scale + shifts[p]
                 act[span, pl.ds(p * block, block)] = jax.nn.silu(normalized).astype(jnp.bfloat16)
             if chunk == order[0]:
+                advance(layer, 2, half_n)
                 for k in range(1, pairs):
                     peer = (q + k) % pairs
                     part = oall.at[layer, pl.ds(pl.multiple_of(peer * block, block), block)]
@@ -362,7 +357,7 @@
         for chunk in order:
             swap_copy(chunk).wait_recv()
 
-            @pl.loop(0, 128 // 32)
+            @pl.loop(0, 128 // 32, unroll=True)
             def _(i, chunk=chunk):
                 span = pl.ds(pl.multiple_of(chunk * 128 + i * 32, 32), 32)
                 branch = (psend[layer, span, :].astype(jnp.float32)
@@ -374,12 +369,9 @@
                     scale = lax.rsqrt(jnp.mean(wide * wide, axis=-1, keepdims=True) + epsilon)
                     normed[span, :] = (wide * scale * gain_ref[pl.ds(layer + 1, 1), :]).astype(jnp.bfloat16)
 
-        for chunk in range(chunks):
-            for k in range(1, m):
-                stat_copy(chunk, k, t).wait_send()
-            conv_copies(1, chunk, q, "wait_send")
-            swap_copy(chunk).wait_send()
-        conv_copies(0, 0, q, "wait_send")
+        for refs, sem in ((stats.at[layer, :, pl.ds(0, m - 1)], ssend), (conv.at[layer, pl.ds(0, pairs - 1)], csend),
+                          (psend.at[layer], xsend)):
+            to_tp(refs, refs, sem.at[layer], xrecv.at[layer, 0], partner).wait_send()
         for kind in range(2):
             pl.when(me < n - 1)(lambda kind=kind: halo_copy(kind).wait_send())
 
@@ -420,21 +412,20 @@
             pltpu.VMEM((HALO, 128), f32),
             pltpu.VMEM((HALO, 128), f32),
             pltpu.VMEM((rows, 128), f32),
-            pltpu.VMEM((layers, m, chunks, 8, 128), f32),
-            pltpu.VMEM((pairs, layers, block), f32),
-            pltpu.VMEM((pairs, layers, block), f32),
+            pltpu.VMEM((layers, chunks, m, 8, 128), f32),
+            pltpu.VMEM((pairs, 2, layers, block), f32),
             pltpu.VMEM((layers, pairs, rows, block), bf16),
             pltpu.VMEM((rows, pairs * block), bf16),
             pltpu.VMEM((layers, rows, width), bf16),
             pltpu.VMEM((layers, rows, width), bf16),
             pltpu.VMEM((max(1, layers - 1), rows, width), bf16),
-            dma((layers, 3)), dma((layers, 3, 2, n // 2, 2)),
+            dma((layers, 3)), dma((layers, 3, n // 2)),
             dma((layers, pairs)), dma((layers, pairs)),
             dma((2 * layers + 1,)), dma((2 * layers + 1,)),
-            dma((layers, m, chunks)), dma((layers, m, chunks)),
-            dma((layers, pairs, chunks + 1)), dma((layers, pairs, chunks + 1)),
-            dma((layers, chunks)), dma((layers, chunks)),
-            dma((pairs, 2)), dma((pairs, 2)), dma((9,)),
+            dma((layers,)), dma((layers, chunks)),
+            dma((layers,)), dma((layers, chunks)),
+            dma((layers,)), dma((layers, chunks)),
+            dma((pairs,)), dma((pairs,)), dma((9,)),
         ],
         compiler_params=pltpu.CompilerParams(
             collective_id=0, has_side_effects=True, vmem_limit_bytes=60 * 1024 * 1024),
@@ -508,7 +499,7 @@
     rows, width = tokens.shape
     depth, block = value_proj.shape[1:]
     return (
-        n % 2 == 0 and 4 <= n <= 16 and m % 2 == 0 and m >= 4 and rows % 128 == 0 and width % 256 == 0
+        n % 2 == 0 and 4 <= n <= 16 and HALO <= GATE_ROWS and m % 2 == 0 and m >= 4 and rows % 128 == 0 and width % 256 == 0
         and depth % 32 == 0 and block == 256 and out_proj.shape[2] % 256 == 0
         and conv_taps.shape[1] - 1 <= HALO
     )

time: 79.2 us -> 76.4 us (0.965)
  Pallas kernels: 77.8 us -> 75.1 us
    pallas_call x1, Pallas kernels: 77.8 us -> 75.1 us  [fused_on_device(): pl.pallas_call(functools.partial(fused_kernel, n, m, reach, layers), out_...]
where the time goes in v4:
time: 76.4 us; the launch traced here: 76.2 us
  Pallas kernels  75.1 us (98%)
  local copies, waits for them, and re-layouts  1.15 us (2%)
    pallas_call x1, Pallas kernels, fused_on_device(): pl.pallas_call(functools.partial(fused_kernel, n, m, reach, layers), out_...  75.1 us

profile of v4, /device:TPU:9, one launch (start us, length us, event | category | flops | bytes accessed | tf_op | source)
XLA Modules:
  0.0 76.2 jit_solution(222496796128497682)
XLA Ops:
  0.0 75.1 %shard_map.91 = bf16[384,2048]{1,0:T(8,128)(2,1)S(1)} custom-call(bf16[384,2048]{1,0:T(8,128)(2,1)} %tok_hbm.1, s32[3,128]{1,0:T(4,128)} %bitcast.3, f32[2,2048]{1,0:T(2,128)} %gain_hbm.1, bf16[2,256,256]{2,1,0:T(8,128)(2,1)} %v_hbm.1, bf16[2,256,256]{2,1,0:T(8,128)(2,1)} %g_hbm.1, bf16[2,256,256]{2,1,0:T(8,128)(2,1)} %o_hbm.1, f32[31,2,256]{2,1,0:T(2,128)} %bitcast.2, ...), custom_call_target="tpu_custom_call" | custom-call | tf_op jit(solution)/shard_map/pallas_call | solution.py:394
  75.1 1.1 %copy.11 = bf16[384,2048]{1,0:T(8,128)(2,1)} copy(bf16[384,2048]{1,0:T(8,128)(2,1)S(1)} %shard_map.91) | data formatting | bytes 3145728

commit v5 on v4

--- a/solution.py
+++ b/solution.py
@@ -224,12 +224,13 @@
                          hsend.at[2 * layer + kind], hrecv.at[2 * layer + kind], following)
 
         def gate_half(kind):
-            acc[...] = jnp.dot(normed[...], w[layer, kind], preferred_element_type=jnp.float32)
+            if layer == 0:
+                acc[kind] = jnp.dot(normed[...], w[layer, kind], preferred_element_type=jnp.float32)
 
             def gate_rows(start):
                 span = pl.ds(start, GATE_ROWS)
-                value = acc[span, pl.ds(0, hb)].astype(jnp.bfloat16).astype(jnp.float32)
-                gate = acc[span, pl.ds(hb, hb)].astype(jnp.bfloat16).astype(jnp.float32)
+                value = acc[kind, span, pl.ds(0, hb)].astype(jnp.bfloat16).astype(jnp.float32)
+                gate = acc[kind, span, pl.ds(hb, hb)].astype(jnp.bfloat16).astype(jnp.float32)
                 gated = (value * jax.nn.sigmoid(gate)).astype(jnp.bfloat16)
                 padded[kind, pl.ds(start + HALO, GATE_ROWS), :] = gated.astype(jnp.float32)
                 return gated
@@ -288,9 +289,29 @@
 
         def first_rows(chunk):
             conv_rows(0, 2 * chunk, 2 * chunk + 2)
-            conv_copies(0, chunk)
-
-        advance(layer, 0, half_n)
+            if not last or chunk == order[0]:
+                conv_copies(0, chunk)
+
+        def absorb(kind, step):
+            for way in range(2 if 0 < step < half_n else 1):
+                owner = owner_at(way, step)
+                span = pl.ds(pl.multiple_of(owner * depth, depth), depth)
+                part = jnp.dot(normed[:, span], w[layer, kind, span, :], preferred_element_type=jnp.float32)
+                acc[kind] = acc[kind] + part if step else part
+
+        def gather(kind):
+            while (layer, kind, half_n) in pending:
+                entry = pending.pop(0)
+                advance_one(*entry)
+                if layer and entry[0] == layer and entry[1] < 2:
+                    absorb(*entry[1:])
+
+        if layer:
+            for step in range(half_n + 1):
+                for kind in range(2):
+                    if (layer, kind, step) not in pending:
+                        absorb(kind, step)
+        gather(0)
         if layer == 0:
             pl.when(me < n - 1)(doc_copy.start)
         gate_half(0)
@@ -301,7 +322,7 @@
         if last:
             for chunk in order[:-1]:
                 first_rows(chunk)
-        advance(layer, 1, half_n)
+        gather(1)
         gate_half(1)
         if not last:
             pause()
@@ -309,13 +330,20 @@
                 first_rows(chunk)
         for chunk in order:
             if chunk == 0:
+                conv_rows(0, 1, 2)
+                conv_rows(1, 1, 2)
                 take_halo(0)
-                first_rows(0)
+                conv_rows(0, 0, 1)
+                conv_copies(0, 0)
                 pause()
                 take_halo(1)
-            conv_rows(1, 2 * chunk, 2 * chunk + 2)
+                conv_rows(1, 0, 1)
+            else:
+                conv_rows(1, 2 * chunk, 2 * chunk + 2)
             stats[layer, chunk, t] = jnp.transpose(stat[pl.ds(chunk * 128, 128), :])[:8]
             stat_copies(chunk)
+            if last and chunk in order[1:-1]:
+                conv_copies(0, chunk)
             conv_copies(1, chunk)
 
         pause()
@@ -403,7 +431,7 @@
             pltpu.VMEM((layers, 2, n * depth, block), bf16),
             pltpu.VMEM((layers, pairs * block, n * owidth), bf16),
             pltpu.VMEM((rows, width), bf16),
-            pltpu.VMEM((rows, block), f32),
+            pltpu.VMEM((2, rows, block), f32),
             pltpu.VMEM((2, rows + HALO, block // 2), f32),
             pltpu.VMEM((rows + HALO, 128), f32),
             pltpu.VMEM((rows, 128), i32),

time: 76.4 us -> 75.7 us (level)
  Pallas kernels: 75.1 us -> 73.9 us
    pallas_call x1, Pallas kernels: 75.1 us -> 73.9 us  [fused_on_device(): pl.pallas_call(functools.partial(fused_kernel, n, m, reach, layers), out_...]
where the time goes in v5:
time: 75.7 us; the launch traced here: 75.1 us
  Pallas kernels  73.9 us (98%)
  local copies, waits for them, and re-layouts  1.15 us (2%)
    pallas_call x1, Pallas kernels, fused_on_device(): pl.pallas_call(functools.partial(fused_kernel, n, m, reach, layers), out_...  73.9 us

profile of v5, /device:TPU:9, one launch (start us, length us, event | category | flops | bytes accessed | tf_op | source)
XLA Modules:
  0.0 75.1 jit_solution(10909106951320382119)
XLA Ops:
  0.0 73.9 %shard_map.91 = bf16[384,2048]{1,0:T(8,128)(2,1)S(1)} custom-call(bf16[384,2048]{1,0:T(8,128)(2,1)} %tok_hbm.1, s32[3,128]{1,0:T(4,128)} %bitcast.3, f32[2,2048]{1,0:T(2,128)} %gain_hbm.1, bf16[2,256,256]{2,1,0:T(8,128)(2,1)} %v_hbm.1, bf16[2,256,256]{2,1,0:T(8,128)(2,1)} %g_hbm.1, bf16[2,256,256]{2,1,0:T(8,128)(2,1)} %o_hbm.1, f32[31,2,256]{2,1,0:T(2,128)} %bitcast.2, ...), custom_call_target="tpu_custom_call" | custom-call | tf_op jit(solution)/shard_map/pallas_call | solution.py:422
  73.9 1.1 %copy.11 = bf16[384,2048]{1,0:T(8,128)(2,1)} copy(bf16[384,2048]{1,0:T(8,128)(2,1)S(1)} %shard_map.91) | data formatting | bytes 3145728

commit v6 on v5

--- a/solution.py
+++ b/solution.py
@@ -77,30 +77,41 @@
             return w.at[layer, kind, pl.ds(0, count * depth)]
         return oall.at[layer, pl.ds(pl.multiple_of(q * block, block), block), pl.ds(0, count * owidth)]
 
-    def ring_copy(layer, kind, way, step, src, dst):
-        return to_sp(src, dst, rsend.at[layer, kind], rrecv.at[layer, kind, step], right if way == 0 else left)
+    def ring_copy(layer, kind, way, slot, src, dst):
+        return to_sp(src, dst, rsend.at[layer, kind], rrecv.at[layer, kind, slot], right if way == 0 else left)
 
     def spread_copy(layer, k, src, dst):
         return to_tp(src, dst, osend.at[layer, k], orecv.at[layer, q], 2 * ((q + k) % pairs) + c)
 
     def advance_one(layer, kind, step):
-        if step > 0:
-            landed = several(layer, kind, 2 if step < half_n else 1)
-            ring_copy(layer, kind, 0, step - 1, landed, landed).wait_recv()
-        for way in range(2):
+        def land(slot, count):
+            landed = several(layer, kind, count)
+            ring_copy(layer, kind, 0, slot, landed, landed).wait_recv()
+
+        def send(way, slot, first, count):
             owner = owner_at(way, step)
-            first, count = (0, 2) if step < half_n - 1 else (way, 1)
-            if step == half_n:
-                continue
             dst = held(layer, kind, owner, first, count)
             if step > 0:
-                ring_copy(layer, kind, way, step, dst, dst).start()
+                ring_copy(layer, kind, way, slot, dst, dst).start()
             elif kind == 2:
-                ring_copy(layer, kind, way, step, o_ref.at[layer, :, pl.ds(first * ho, count * ho)], dst).start()
+                ring_copy(layer, kind, way, slot, o_ref.at[layer, :, pl.ds(first * ho, count * ho)], dst).start()
             else:
                 for piece in range(first, first + count):
-                    ring_copy(layer, kind, way, step, (v_ref, g_ref)[piece].at[layer, :, pl.ds(kind * hb, hb)],
+                    ring_copy(layer, kind, way, slot, (v_ref, g_ref)[piece].at[layer, :, pl.ds(kind * hb, hb)],
                               held(layer, kind, owner, piece, 1)).start()
+
+        if step > 0:
+            land(step - 1, 2 if step < half_n - 1 else 1)
+        for way in range(2):
+            if step < half_n - 2:
+                send(way, step, 0, 2)
+            elif step < half_n:
+                send(way, step, way, 1)
+        if step == half_n - 2:
+            for way in range(2):
+                send(way, half_n, 1 - way, 1)
+        if step == half_n - 1:
+            land(half_n, 1)
         if kind == 2 and step > 0:
             for way in range(2 if step < half_n else 1):
                 for k in range(1, pairs):
@@ -111,7 +122,7 @@
     for layer in range(layers):
         for step in range(half_n + 1):
             for kind, (first, base, pace) in enumerate(
-                    ((12.2, 11.7, 3.2), (12.3, 12.7, 3.2), (10.5, 11.2, 2.9)) if layer
+                    ((12.2, 11.7, 3.2), (13.3, 12.7, 3.2), (10.5, 10.55, 2.65)) if layer
                     else ((0, 0, 3), (1, 1, 3), (0.5, 0.5, 3))):
                 shift = 11.5 * max(layer - 1, 0)
                 entries.append((shift + (base + pace * step if step else first), layer, kind, step))
@@ -447,7 +458,7 @@
             pltpu.VMEM((layers, rows, width), bf16),
             pltpu.VMEM((layers, rows, width), bf16),
             pltpu.VMEM((max(1, layers - 1), rows, width), bf16),
-            dma((layers, 3)), dma((layers, 3, n // 2)),
+            dma((layers, 3)), dma((layers, 3, n // 2 + 1)),
             dma((layers, pairs)), dma((layers, pairs)),
             dma((2 * layers + 1,)), dma((2 * layers + 1,)),
             dma((layers,)), dma((layers, chunks)),

time: 75.7 us -> 75.3 us (level)
  no operation moved by 1% of the time
where the time goes in v6:
time: 75.3 us; the launch traced here: 74.8 us
  Pallas kernels  73.7 us (98%)
  local copies, waits for them, and re-layouts  1.15 us (2%)
    pallas_call x1, Pallas kernels, fused_on_device(): pl.pallas_call(functools.partial(fused_kernel, n, m, reach, layers), out_...  73.7 us

profile of v6, /device:TPU:9, one launch (start us, length us, event | category | flops | bytes accessed | tf_op | source)
XLA Modules:
  0.0 74.8 jit_solution(9164105929797000876)
XLA Ops:
  0.0 73.7 %shard_map.91 = bf16[384,2048]{1,0:T(8,128)(2,1)S(1)} custom-call(bf16[384,2048]{1,0:T(8,128)(2,1)} %tok_hbm.1, s32[3,128]{1,0:T(4,128)} %bitcast.3, f32[2,2048]{1,0:T(2,128)} %gain_hbm.1, bf16[2,256,256]{2,1,0:T(8,128)(2,1)} %v_hbm.1, bf16[2,256,256]{2,1,0:T(8,128)(2,1)} %g_hbm.1, bf16[2,256,256]{2,1,0:T(8,128)(2,1)} %o_hbm.1, f32[31,2,256]{2,1,0:T(2,128)} %bitcast.2, ...), custom_call_target="tpu_custom_call" | custom-call | tf_op jit(solution)/shard_map/pallas_call | solution.py:433
  73.7 1.1 %copy.11 = bf16[384,2048]{1,0:T(8,128)(2,1)} copy(bf16[384,2048]{1,0:T(8,128)(2,1)S(1)} %shard_map.91) | data formatting | bytes 3145728
